TPU v7x, 512 devices: a whole 4x8x8 slice. The times are simulated.
512 devices in a mesh: gr: 2 (over z_hi), sp: 32 (over z_lo, y), tp: 8 (over x, core).
Axes of the slice: x: 4, y: 8, z: 8 (z_hi: 2, z_lo: 4; z = z_hi * 4 + z_lo), core: 2. Of those that a mesh axis runs over, the one named last changes fastest.
Arguments:
- prompt_elements: bfloat16 [4, 8192, 2048], P('gr', 'sp'), may hold values from -6 to 6
- address_weights: bfloat16 [2048, 1024], P(None, 'tp'), may hold values from -0.125 to 0.125
- content_weights: bfloat16 [2048, 1024], P(None, 'tp'), may hold values from -0.125 to 0.125
- lookup_weights: bfloat16 [2048, 1024], P(None, 'tp'), may hold values from -0.125 to 0.125
- forgetting_weights: bfloat16 [2048, 8], replicated, may hold values from -0.125 to 0.125
- update_intensity_weights: bfloat16 [2048, 8], replicated, may hold values from -0.125 to 0.125
- forgetting_speeds: float32 [8], P('tp'), may hold values from 1.2207031e-05 to 0.05, as said below
- update_intensity_ceiling: float32 [8], P('tp'), may hold values from 0.0078125 to 0.03125, as said below
- forgetting_multiplier: float32 [4, 8192, 8], P('gr', 'sp', 'tp'), may hold values from 0.35 to 2.8, as said below
- spike_offsets: float32 [4, 8192, 8], P('gr', 'sp', 'tp'), may hold values from -0.7 to 0, as said below
- upcoming_element_vector: bfloat16 [4, 2048], P('gr'), may hold values from -6 to 6
- retrieval_rms_multiplier: float32 [128], replicated, may hold values from 0.1 to 1.9
Outputs:
- cache: bfloat16 [4, 8, 128, 128], P('gr', 'tp', 'sp')
- read: bfloat16 [4, 1024], P('gr', 'tp')
Inputs may be any that keep to these rules, and one draw needn't show every extreme that they name: `forgetting_speeds`: per-head rates of decay. `update_intensity_ceiling`: per-head strength scales. `forgetting_multiplier`: positive factors. `spike_offsets`: non-positive log factors.
All inputs are finite; a program needn't handle non-finite values.
Results may differ from a plain program's by a relative error of at most 0.0037.
Values sent between devices are 32-bit elements; how exact they have to be, the bound alone decides.
A program may use at most 64 MiB of HBM per device.

v0:
```python
import jax
import jax.numpy as jnp
from jax import lax
from jax.sharding import Mesh
from jax.sharding import PartitionSpec as P

BLK = 64
SP = ("sp_0", "sp_1")


HIGH = lax.Precision.HIGHEST
EPS = 1e-06


def filled_with(x, identity):
    return jnp.broadcast_to(jnp.asarray(identity, x.dtype), x.shape)


def carried_in(x, axes, combine, identity):
    before = start = filled_with(x, identity)
    subtotal = x
    for axis in reversed(axes):
        size, index = (lax.axis_size(axis), lax.axis_index(axis))
        pieces = lax.all_gather(subtotal, axis)
        inside, subtotal = (start, start)
        for k in reversed(range(size)):
            passed = k > index
            subtotal = combine(subtotal, pieces[k])
            inside = jnp.where(passed, subtotal, inside)
        before = combine(inside, before)
    return before


def split_up(x, dim, size):
    before, after = (x.shape[:dim], x.shape[dim + 1 :])
    return jnp.moveaxis(x.reshape(*before, size, -1, *after), dim, 0)


def sum_at_owner(x, axis, dim):
    size = lax.axis_size(axis)
    tiles = lax.all_to_all(split_up(x, dim, size), axis, 0, 0, tiled=True)
    return jnp.sum(tiles, axis=0)


def by_axis(x, axes):
    for axis in axes:
        x = lax.psum(x, axis)
    return x


def silu_f(values):
    return values * jax.nn.sigmoid(values)


def unit_rows(values):
    return values * lax.rsqrt(jnp.sum(values * values, axis=-1, keepdims=True) + EPS)


def unit_inverse(lower):
    eye = jnp.eye(lower.shape[-1], dtype=jnp.float32)
    power = -lower
    result = eye + power
    degree = 2
    while degree < lower.shape[-1]:
        power = jnp.matmul(power, power, precision=HIGH)
        result = jnp.matmul(result, eye + power, precision=HIGH)
        degree = degree * 2
    return result


def head_inputs(
    flat,
    address_weights,
    content_weights,
    decay_cols,
    strength_cols,
    forgetting_speeds,
    update_intensity_ceiling,
    head_dim,
):
    count = flat.shape[0]
    key_raw = lax.optimization_barrier(
        jnp.dot(flat, address_weights, preferred_element_type=jnp.float32).astype(jnp.bfloat16)
    )
    value_raw = lax.optimization_barrier(
        jnp.dot(flat, content_weights, preferred_element_type=jnp.float32).astype(jnp.bfloat16)
    )
    keys = unit_rows(silu_f(key_raw.astype(jnp.float32)).reshape(count, -1, head_dim))
    values = silu_f(value_raw.astype(jnp.float32)).reshape(count, -1, head_dim)
    decay_pre = jnp.dot(flat, decay_cols, preferred_element_type=jnp.float32)
    strength_pre = jnp.dot(flat, strength_cols, preferred_element_type=jnp.float32)
    speed_addend = -forgetting_speeds * jax.nn.softplus(decay_pre)
    strength = update_intensity_ceiling * jax.nn.sigmoid(strength_pre)
    return (keys, values, speed_addend, strength)


def to_blocks(values, seqs):
    shaped = values.reshape((seqs, -1) + values.shape[1:])
    moved = jnp.moveaxis(shaped, 2, 1)
    return moved.reshape((moved.shape[0] * moved.shape[1], -1, BLK) + moved.shape[3:])


def block_terms(keys, values, forgetting_exponent, strength):
    size = keys.shape[2]
    cumulative = jnp.cumsum(forgetting_exponent, axis=-1)
    places = jnp.arange(size)
    inclusive = places[:, None] >= places[None, :]
    strict = places[:, None] > places[None, :]
    spread = jnp.where(inclusive, cumulative[..., :, None] - cumulative[..., None, :], -jnp.inf)
    weighted = keys * strength[..., None]
    lower = jnp.where(
        strict, jnp.einsum("gncd,gnmd->gncm", weighted, keys, precision=HIGH) * jnp.exp(spread), 0.0
    )
    solved = unit_inverse(lower)
    targets = jnp.matmul(solved, values * strength[..., None], precision=HIGH)
    erasers = jnp.matmul(solved, weighted * jnp.exp(cumulative)[..., None], precision=HIGH)
    final_log = cumulative[..., -1]
    faded = keys * jnp.exp(final_log[..., None] - cumulative)[..., None]
    return (targets, erasers, faded, final_log)


def finish(
    query, keys, values, speed_addend, strength, query_state, key_state, retrieval_rms_multiplier
):
    match = jnp.sum(query * keys, axis=-1) * strength
    fading = jnp.exp(speed_addend)
    mixed = (
        fading[..., None] * (query_state - match[..., None] * key_state) + match[..., None] * values
    )
    scaled = (
        mixed
        * lax.rsqrt(jnp.mean(mixed * mixed, axis=-1, keepdims=True) + EPS)
        * retrieval_rms_multiplier
    )
    return scaled.reshape(scaled.shape[0], -1).astype(jnp.bfloat16)


def new_query(upcoming_element_vector, lookup_weights, head_dim):
    query_raw = lax.optimization_barrier(
        jnp.dot(upcoming_element_vector, lookup_weights, preferred_element_type=jnp.float32).astype(
            jnp.bfloat16
        )
    )
    query = unit_rows(
        silu_f(query_raw.astype(jnp.float32)).reshape(
            upcoming_element_vector.shape[0], -1, head_dim
        )
    )
    return query * head_dim ** (-0.5)


def compose(left_map, right_map):
    return jnp.einsum("shij,shjk->shik", left_map, right_map, precision=HIGH)


def on_device(
    prompt_elements,
    address_weights,
    content_weights,
    lookup_weights,
    forgetting_weights,
    update_intensity_weights,
    forgetting_speeds,
    update_intensity_ceiling,
    forgetting_multiplier,
    spike_offsets,
    upcoming_element_vector,
    retrieval_rms_multiplier,
):
    seqs, span, width = prompt_elements.shape
    head_dim = retrieval_rms_multiplier.shape[0]
    shard_attention_groups = forgetting_speeds.shape[0]
    first_head = lax.axis_index("tp") * shard_attention_groups
    decay_cols = lax.dynamic_slice_in_dim(forgetting_weights, first_head, shard_attention_groups, 1)
    strength_cols = lax.dynamic_slice_in_dim(
        update_intensity_weights, first_head, shard_attention_groups, 1
    )
    flat = prompt_elements.reshape(seqs * span, width)
    keys, values, speed_addend, strength = head_inputs(
        flat,
        address_weights,
        content_weights,
        decay_cols,
        strength_cols,
        forgetting_speeds,
        update_intensity_ceiling,
        head_dim,
    )
    forgetting_exponent = speed_addend * forgetting_multiplier.reshape(
        -1, shard_attention_groups
    ) + spike_offsets.reshape(-1, shard_attention_groups)
    targets, erasers, faded, final_log = block_terms(
        to_blocks(keys, seqs),
        to_blocks(values, seqs),
        to_blocks(forgetting_exponent, seqs),
        to_blocks(strength, seqs),
    )
    groups = seqs * shard_attention_groups
    eye = jnp.eye(head_dim, dtype=jnp.float32)
    carry_a = jnp.broadcast_to(eye, (groups, head_dim, head_dim))
    carry_b = jnp.zeros((groups, head_dim, head_dim), jnp.float32)
    for index in range(span // BLK):
        fade_t = jnp.swapaxes(faded[:, index], -1, -2)
        block_a = jnp.exp(final_log[:, index])[:, None, None] * eye - jnp.matmul(
            fade_t, erasers[:, index], precision=HIGH
        )
        block_b = jnp.matmul(fade_t, targets[:, index], precision=HIGH)
        carry_a = jnp.matmul(block_a, carry_a, precision=HIGH)
        carry_b = jnp.matmul(block_a, carry_b, precision=HIGH) + block_b
    map_shape = (seqs, shard_attention_groups, head_dim, head_dim)
    carry_a = carry_a.reshape(map_shape)
    carry_b = carry_b.reshape(map_shape)
    query = new_query(upcoming_element_vector, lookup_weights, head_dim)
    new_keys, new_values, rate_new, strength_new = head_inputs(
        upcoming_element_vector,
        address_weights,
        content_weights,
        decay_cols,
        strength_cols,
        forgetting_speeds,
        update_intensity_ceiling,
        head_dim,
    )
    rows = head_dim // lax.axis_size(SP)
    row_start = lax.axis_index(SP) * rows
    unit_map = jnp.broadcast_to(eye, map_shape)

    def onward_map(earlier, later):
        return compose(earlier, later)

    after = carried_in(carry_a, SP, onward_map, unit_map)
    own_rows = sum_at_owner(compose(after, carry_b), SP, 2)
    query_rows = lax.dynamic_slice_in_dim(query, row_start, rows, 2)
    key_rows = lax.dynamic_slice_in_dim(new_keys, row_start, rows, 2)
    query_part = jnp.einsum("shk,shkv->shv", query_rows, own_rows, precision=HIGH)
    key_part = jnp.einsum("shk,shkv->shv", key_rows, own_rows, precision=HIGH)
    cache = own_rows.astype(jnp.bfloat16)
    query_state, key_state = (by_axis(query_part, SP), by_axis(key_part, SP))
    read = finish(
        query,
        new_keys,
        new_values,
        rate_new,
        strength_new,
        query_state,
        key_state,
        retrieval_rms_multiplier,
    )
    return (cache, read)


def solution(mesh):
    split = Mesh(
        mesh.devices.reshape(mesh.shape["gr"], 4, 8, mesh.shape["tp"]), ("gr", "sp_0", "sp_1", "tp")
    )
    placed = (
        P("gr", SP, None),
        P(None, "tp"),
        P(None, "tp"),
        P(None, "tp"),
        P(),
        P(),
        P("tp"),
        P("tp"),
        P("gr", SP, "tp"),
        P("gr", SP, "tp"),
        P("gr", None),
        P(),
    )
    return jax.shard_map(
        on_device,
        mesh=split,
        in_specs=placed,
        out_specs=(P("gr", "tp", SP, None), P("gr", "tp")),
        check_vma=False,
    )
```

profile of v0, /device:TPU:6, one launch (start us, length us, event | category | flops | bytes accessed | tf_op | source)
XLA Modules:
  0.0 147.7 jit_solution(15972106579119152718)
XLA Ops:
  8.1 0.7 copy-done
  8.8 1.5 fusion.87
  10.4 0.5 reduce_window_sum.11
  11.1 0.2 exponential_reduce_fusion
  11.3 0.6 fusion.84
  12.7 0.7 convolution_convert_fusion.1
  13.8 0.6 fusion.1
  14.4 0.4 fusion.115
  14.8 0.4 fusion.116
  15.2 0.4 fusion.24
  15.6 0.4 fusion.117
  16.0 0.4 fusion.22
  16.4 0.4 fusion.118
  16.8 0.4 fusion.20
  17.2 0.4 convolution_add_fusion
  17.6 0.4 fusion.18
  18.1 0.4 fusion.119
  18.5 0.5 fusion.15
  19.1 0.4 convolution_subtract_fusion
  19.5 0.4 convolution_subtract_fusion.1
  19.9 0.4 convolution_subtract_fusion.2
  20.3 0.4 convolution_subtract_fusion.3
  20.7 0.3 fusion.72
  21.0 0.3 fusion.120
  21.3 0.3 fusion.121
  21.5 0.9 fusion.122
  22.5 1.8 %fusion.67 = f32[2,128,128]{2,1,0:T(8,128)} fusion(f32[2,128,128]{2,1,0:T(8,128)} %copy-done.4), kind=kOutput, calls=%fused_computation.106 | convolution fusion | flops 50331648 | bytes 262144 | tf_op jit(solution)/shard_map/dot_general | solution.py:209
  24.4 0.9 fusion.110
  25.4 1.8 %convolution_convert_fusion = bf16[512,128]{1,0:T(8,128)(2,1)S(1)} fusion(bf16[512,2048]{1,0:T(8,128)(2,1)S(1)} %bitcast.163, bf16[2048,128]{1,0:T(8,128)(2,1)} %param.14), kind=kOutput, calls=%fused_computation.4 | convolution fusion | flops 268500992 | bytes 2752512 | tf_op jit(solution)/shard_map/dot_general | solution.py:86
  27.2 1.2 fusion.16
  28.5 1.2 convolution_convert_fusion.4
  29.9 2.0 %convolution_add_fusion.4 = f32[2,128,128]{2,1,0:T(8,128)} fusion(f32[2,128,128]{2,1,0:T(8,128)} %fusion.67, f32[2,4,64,128]{3,2,1,0:T(8,128)} %fusion.16, f32[2,4,64,128]{3,2,0,1:T(8,128)S(1)} %copy_multiply_fusion), kind=kOutput, calls=%fused_computation.9 | convolution fusion | flops 25198592 | bytes 393216 | tf_op jit(solution)/shard_map/dot_general | solution.py:207
  31.9 0.2 multiply_reduce_fusion.2
  32.1 1.2 fusion.124
  33.3 1.2 convolution_add_fusion.3
  34.6 0.3 fusion.125
  34.9 0.4 convolution_add_fusion.2
  35.3 0.3 fusion.126
  35.5 0.4 convolution_add_fusion.1
  36.1 31.7 %all-gather.4.cloned.1.call-done = f32[16,128,128]{2,1,0:T(8,128)} async-done(((f32[2,128,128]{2,1,0:T(8,128)}), f32[16,128,128]{2,1,0:T(8,128)}) %all-gather.4.cloned.1.call-update) | async-done | bytes 1048592 | tf_op jit(solution)/shard_map/all_gather | solution.py:24
  67.8 1.2 fusion.48
  69.0 1.2 fusion.46
  70.2 1.4 fusion.44
  71.5 1.2 fusion.42
  72.7 1.2 fusion.40
  73.9 1.2 fusion.38
  75.1 1.2 fusion.36
  76.2 1.2 fusion.34
  77.4 16.5 %all-gather.1 = f32[8,128,128]{2,1,0:T(8,128)S(1)} all-gather(f32[2,128,128]{2,1,0:T(8,128)S(1)} %fusion.34), channel_id=3, replica_groups=mesh['gr'=2,'sp_0'=4,'sp_1'=8,'tp'=8] {'sp_0'}, dimensions={0}, use_global_device_ids=true | all-gather | bytes 655360 | tf_op jit(solution)/shard_map/all_gather | solution.py:24
  93.9 0.3 fusion.32
  94.2 0.3 fusion.30
  94.5 0.3 fusion.28
  94.8 0.3 convolution_select_fusion
  95.1 0.3 fusion.50
  95.4 0.3 fusion.123
  95.6 0.3 fusion.127
  95.9 0.7 copy.27
  96.6 7.6 %all-to-all-start = ((f32[32,2,1,4,128]{4,3,1,2,0:T(4,128)}), f32[32,2,1,4,128]{4,3,1,2,0:T(4,128)S(1)}, u32[]{:S(2)}, u32[]{:S(2)}) async-start(f32[32,2,1,4,128]{4,3,1,2,0:T(4,128)} %bitcast.157), calls=%async_computation | async-start | bytes 262144 | tf_op jit(solution)/shard_map/all_to_all | solution.py:41
  104.4 10.3 %all-to-all-done = f32[32,2,1,4,128]{4,3,1,2,0:T(4,128)S(1)} async-done(((f32[32,2,1,4,128]{4,3,1,2,0:T(4,128)}), f32[32,2,1,4,128]{4,3,1,2,0:T(4,128)S(1)}, u32[]{:S(2)}, u32[]{:S(2)}) %all-to-all-start) | async-done | bytes 131104 | tf_op jit(solution)/shard_map/all_to_all | solution.py:41
  114.7 0.6 convert_bitcast_fusion
  115.6 9.5 %all-reduce.1 = (f32[2,1,128]{2,0,1:T(2,128)S(1)}, f32[2,1,128]{2,0,1:T(2,128)S(1)}) all-reduce(f32[2,1,128]{2,0,1:T(2,128)S(1)} %bitcast.174, f32[2,1,128]{2,0,1:T(2,128)S(1)} %bitcast.173), channel_id=1, replica_groups=mesh['gr'=2,'sp_0'=4,'sp_1'=8,'tp'=8] {'sp_0'}, use_global_device_ids=true, to_apply=%region_4.5 | all-reduce | flops 512 | bytes 4096 | tf_op jit(solution)/shard_map/psum | solution.py:47
  125.1 15.0 %all-reduce = (f32[2,1,128]{2,0,1:T(2,128)S(1)}, f32[2,1,128]{2,0,1:T(2,128)S(1)}) all-reduce(f32[2,1,128]{2,0,1:T(2,128)S(1)} %get-tuple-element.8, f32[2,1,128]{2,0,1:T(2,128)S(1)} %get-tuple-element.9), channel_id=1, replica_groups=mesh['gr'=2,'sp_0'=4,'sp_1'=8,'tp'=8] {'sp_1'}, use_global_device_ids=true, to_apply=%region_5.6 | all-reduce | flops 512 | bytes 4096 | tf_op jit(solution)/shard_map/psum | solution.py:47
  140.1 0.2 multiply_reduce_fusion.1
  140.3 0.6 fusion.106
  (50 shorter events, 2.2 us)
Async XLA Ops:
  7.2 1.6 %copy-start = (bf16[2,256,2048]{2,1,0:T(8,128)(2,1)S(1)}, bf16[2,256,2048]{2,1,0:T(8,128)(2,1)}, u32[]{:S(2)}) copy-start(bf16[2,256,2048]{2,1,0:T(8,128)(2,1)} %param.12) | copy-start | bytes 6291460
  7.2 3.1 %copy-start.9 = (f32[2,256,1]{1,2,0:T(1,128)S(1)}, f32[2,256,1]{1,2,0:T(1,128)}, u32[]{:S(2)}) copy-start(f32[2,256,1]{1,2,0:T(1,128)} %param.20) | copy-start | bytes 6148
  7.2 3.1 %copy-start.8 = (f32[2,256,1]{1,2,0:T(1,128)S(1)}, f32[2,256,1]{1,2,0:T(1,128)}, u32[]{:S(2)}) copy-start(f32[2,256,1]{1,2,0:T(1,128)} %param.21) | copy-start | bytes 6148
  7.2 4.1 %copy-start.7 = (bf16[2048,8]{0,1:T(8,128)(2,1)S(1)}, bf16[2048,8]{0,1:T(8,128)(2,1)}, u32[]{:S(2)}) copy-start(bf16[2048,8]{0,1:T(8,128)(2,1)} %param.17) | copy-start | bytes 98308
  7.2 60.6 %all-gather.4.cloned.1.call-start = ((), (), s32[]{:S(2)}) async-start(), calls=%async_computation.1 | async-start | bytes 1179648 | tf_op jit(solution)/shard_map/all_gather | solution.py:24
  8.8 4.0 %copy-start.1 = (bf16[2048,128]{1,0:T(8,128)(2,1)S(1)}, bf16[2048,128]{1,0:T(8,128)(2,1)}, u32[]{:S(2)}) copy-start(bf16[2048,128]{1,0:T(8,128)(2,1)} %param.13) | copy-start | bytes 1572868
  18.5 5.8 %copy-start.6 = (bf16[2,2048]{1,0:T(2,128)(2,1)S(1)}, bf16[2,2048]{1,0:T(2,128)(2,1)}, u32[]{:S(2)}) copy-start(bf16[2,2048]{1,0:T(2,128)(2,1)} %param.22) | copy-start | bytes 24580
  19.5 1.8 %copy-start.4 = (f32[2,128,128]{2,1,0:T(8,128)}, f32[2,128,128]{2,1,0:T(8,128)S(1)}, u32[]{:S(2)}) copy-start(f32[2,128,128]{2,1,0:T(8,128)S(1)} %convolution_subtract_fusion) | copy-start | bytes 393220
  19.9 1.1 copy-start.3
  27.2 8.7 %copy-start.2 = (bf16[2048,128]{1,0:T(8,128)(2,1)S(1)}, bf16[2048,128]{1,0:T(8,128)(2,1)}, u32[]{:S(2)}) copy-start(bf16[2048,128]{1,0:T(8,128)(2,1)} %param.14) | copy-start | bytes 1572868
  28.4 6.4 %copy-start.5 = (f32[2,4,64,128]{3,2,1,0:T(8,128)S(1)}, f32[2,4,64,128]{3,2,1,0:T(8,128)}, u32[]{:S(2)}) copy-start(f32[2,4,64,128]{3,2,1,0:T(8,128)} %fusion.16) | copy-start | bytes 786436
  94.5 45.8 %copy-start.10 = (f32[128]{0:T(128)S(1)}, f32[128]{0:T(128)}, u32[]{:S(2)}) copy-start(f32[128]{0:T(128)} %param.23) | copy-start | bytes 1540
  96.6 18.1 %all-to-all-start = ((f32[32,2,1,4,128]{4,3,1,2,0:T(4,128)}), f32[32,2,1,4,128]{4,3,1,2,0:T(4,128)S(1)}, u32[]{:S(2)}, u32[]{:S(2)}) async-start(f32[32,2,1,4,128]{4,3,1,2,0:T(4,128)} %bitcast.157), calls=%async_computation | async-start | bytes 262144 | tf_op jit(solution)/shard_map/all_to_all | solution.py:41
Sparse Core Ops, SparseCore 0:
  22.6 45.1 all-gather.3
where the time goes:
time: 148 us
  waiting for transfers between devices  42 us (28%)
  blocking collectives  41.1 us (28%)
  matrix products  36 us (24%)
  between operations  16 us (11%)
  starting transfers between devices  7.62 us (5%)
  other arithmetic  2.99 us (2%)
  local copies, waits for them, and re-layouts  2.06 us (1%)
    all_gather x1, waiting for transfers between devices, carried_in(): pieces = lax.all_gather(subtotal, axis)  31.7 us
    psum x2, blocking collectives, by_axis(): x = lax.psum(x, axis)  24.5 us
    all_gather x1, blocking collectives, carried_in(): pieces = lax.all_gather(subtotal, axis)  16.5 us
    dot_general x15, matrix products, compose(): return jnp.einsum('shij,shjk->shik', left_map, right_map, precision=HIGH)  11.5 us
    all_to_all x1, waiting for transfers between devices, sum_at_owner(): tiles = lax.all_to_all(split_up(x, dim, size), axis, 0, 0, tiled=True)  10.3 us
    all_to_all x1, starting transfers between devices, sum_at_owner(): tiles = lax.all_to_all(split_up(x, dim, size), axis, 0, 0, tiled=True)  7.58 us
    dot_general x4, matrix products, on_device(): block_b = jnp.matmul(fade_t, targets[:, index], precision=HIGH)  4 us
    dot_general x4, matrix products, on_device(): carry_b = jnp.matmul(block_a, carry_b, precision=HIGH) + block_b  3.57 us
  transfers between devices with their start and end apart: 2, of which 2 were waited for; matrix products, arithmetic and copies ran while one was open for 9% of the time, Pallas kernels for 0%

commit v1 on v0

v1 whole, which is shorter than its diff:
```python
import jax
import jax.numpy as jnp
from jax import lax
from jax.experimental import pallas as pl
from jax.experimental.pallas import tpu as pltpu
from jax.sharding import PartitionSpec as P

EPS = 1e-06
F32 = jnp.float32
BF16 = jnp.bfloat16
MESH = pl.DeviceIdType.MESH
NY = 8
NZ = 4
N = NY * NZ
CH = 128
HD = 128
NN = (((1,), (0,)), ((), ()))
NT = (((1,), (1,)), ((), ()))


def dot1(a, b, dims=NN):
    return lax.dot_general(a.astype(BF16), b.astype(BF16), dims, preferred_element_type=F32)


def halves(a):
    high = a.astype(BF16)
    return high, (a - high.astype(F32)).astype(BF16)


def dot3(a, b):
    ah, al = halves(a)
    bh, bl = halves(b)
    left = jnp.concatenate([ah, ah, al], axis=1)
    right = jnp.concatenate([bh, bl, bh], axis=0)
    return lax.dot_general(left, right, NN, preferred_element_type=F32)


def silu(z):
    return z / (1.0 + jnp.exp(-z))


def softplus(z):
    return jnp.maximum(z, 0.0) + jnp.log1p(jnp.exp(-jnp.abs(z)))


def sigmoid(z):
    return 1.0 / (1.0 + jnp.exp(-z))


def unit_rows(z):
    return z * lax.rsqrt(jnp.sum(z * z, axis=-1, keepdims=True) + EPS)


def iota(shape, dim):
    return lax.broadcasted_iota(jnp.int32, shape, dim)


def compose(early, late_a, late_b):
    moved = dot3(early, late_a)
    return moved[:HD], moved[HD:] + late_b


def chunk_map(k, v, c, beta):
    rows, cols = iota((CH, CH), 0), iota((CH, CH), 1)
    c_cols = jnp.broadcast_to(c, (CH, CH))
    c_rows = jnp.transpose(c_cols)
    end = c[:, CH - 1 :]
    match = dot1(k, k, NT)
    power = jnp.where(cols > rows, match * beta * jnp.exp(c_cols - c_rows), 0.0)
    k_t, v_t = jnp.transpose(k), jnp.transpose(v)
    rhs = jnp.concatenate([k_t * (-beta * jnp.exp(c)), v_t * beta], axis=0)
    both = dot1(jnp.concatenate([rhs, power], axis=0), power)
    rhs = rhs - both[: 2 * HD]
    power = both[2 * HD :]
    for _ in range(5):
        both = dot1(jnp.concatenate([rhs, power], axis=0), power)
        rhs = rhs + both[: 2 * HD]
        power = both[2 * HD :]
    rhs = rhs + dot1(rhs, power)
    faded = k * jnp.exp(end - c_rows)
    out = dot3(rhs, faded)
    return out[:HD] + jnp.where(rows == cols, jnp.exp(end), 0.0), out[HD:]


def kernel(
    x_hbm,
    wk_hbm,
    wv_hbm,
    wq_hbm,
    wf_hbm,
    wu_hbm,
    speed_ref,
    ceil_ref,
    mult_hbm,
    spike_hbm,
    up_hbm,
    gain_hbm,
    cache_ref,
    read_ref,
    xs,
    wkv,
    wqs,
    wfs,
    wus,
    mults,
    spikes,
    ups,
    gains,
    dsc,
    uq,
    uk,
    other_map,
    own_map,
    pair_map,
    row_map,
    row_sum,
    col_map,
    msg,
    fin,
    lsem,
    s1,
    r1,
    s2,
    r2,
    s3,
    r3,
    s4,
    r4,
):
    sp = lax.axis_index("sp")
    tp = lax.axis_index("tp")
    y, z = sp % NY, sp // NY
    core = tp % 2
    par, pair = y % 2, y // 2
    turned = (pair - core + 4) % 4
    s = (par + (turned + 1) // 2) % 2
    other = 1 - s
    vy = (y - 2 * core + NY) % NY
    half = vy % 4 - 1
    is_rx = (vy % 4 == 1) | (vy % 4 == 2)
    head = tp % wf_hbm.shape[0]

    def rx_y(seq, c):
        return ((1 - seq) * 4 + 1 + c + 2 * core) % NY

    loads = [
        pltpu.make_async_copy(wk_hbm, wkv.at[:, 0:HD], lsem.at[0]),
        pltpu.make_async_copy(wv_hbm, wkv.at[:, HD : 2 * HD], lsem.at[1]),
        pltpu.make_async_copy(x_hbm.at[other], xs.at[other], lsem.at[2]),
        pltpu.make_async_copy(wf_hbm, wfs, lsem.at[3]),
        pltpu.make_async_copy(wu_hbm, wus, lsem.at[4]),
        pltpu.make_async_copy(mult_hbm, mults, lsem.at[5]),
        pltpu.make_async_copy(spike_hbm, spikes, lsem.at[6]),
        pltpu.make_async_copy(x_hbm.at[s], xs.at[s], lsem.at[7]),
        pltpu.make_async_copy(wq_hbm, wqs, lsem.at[8]),
        pltpu.make_async_copy(up_hbm, ups, lsem.at[9]),
        pltpu.make_async_copy(gain_hbm, gains, lsem.at[10]),
    ]
    for load in loads:
        load.start()

    barrier = pltpu.get_barrier_semaphore()
    for i in range(1, N):
        pl.semaphore_signal(
            barrier, inc=1, device_id={"sp": (sp + i) % N}, device_id_type=MESH
        )

    speed = speed_ref[0]
    ceiling = ceil_ref[0]
    for i in range(7):
        loads[i].wait()
    w_all = wkv[...]
    wfu = jnp.concatenate([wfs[...].astype(F32), wus[...].astype(F32)], axis=0).astype(BF16)
    heads = wf_hbm.shape[0]

    def seq_map(seq):
        x = xs[seq]
        raw = lax.dot_general(x, w_all, NN, preferred_element_type=F32)
        raw = raw.astype(BF16).astype(F32)
        act = silu(raw)
        k, v = unit_rows(act[:, :HD]), act[:, HD:]
        dsc[...] = lax.dot_general(wfu, x, NT, preferred_element_type=F32)
        decay = dsc[pl.ds(head, 1), :]
        strength = dsc[pl.ds(heads + head, 1), :]
        g = -speed * softplus(decay) * mults[seq] + spikes[seq]
        beta = ceiling * sigmoid(strength)
        g_high = g.astype(BF16).astype(F32)
        g_rest = g - g_high
        g_mid = g_rest.astype(BF16).astype(F32)
        g_low = g_rest - g_mid
        row = iota((8, CH), 0)
        parts = jnp.zeros((8, CH), F32)
        place = 0
        for i in range(2):
            for part in (g_high, g_mid, g_low):
                parts = jnp.where(row == place, part[:, i * CH : (i + 1) * CH], parts)
                place += 1
        upper = jnp.where(iota((CH, CH), 0) <= iota((CH, CH), 1), 1.0, 0.0)
        sums = dot1(parts, upper)
        maps = []
        for i in range(2):
            c = sums[3 * i : 3 * i + 1] + sums[3 * i + 1 : 3 * i + 2] + sums[3 * i + 2 : 3 * i + 3]
            sl = slice(i * CH, (i + 1) * CH)
            maps.append(chunk_map(k[sl], v[sl], c, beta[:, sl]))
        early = jnp.concatenate(maps[0], axis=0)
        return compose(early, maps[1][0], maps[1][1])

    a, b = seq_map(other)
    other_map[0:HD] = a
    other_map[HD : 2 * HD] = b
    pl.semaphore_wait(barrier, N - 1)
    partner = sp + 1 - 2 * par
    swap = pltpu.make_async_remote_copy(
        src_ref=other_map,
        dst_ref=own_map.at[par],
        send_sem=s1,
        recv_sem=r1,
        device_id={"sp": partner},
        device_id_type=MESH,
    )
    swap.start()
    loads[7].wait()
    a, b = seq_map(s)
    own_map[par, 0:HD] = a
    own_map[par, HD : 2 * HD] = b
    pltpu.make_async_remote_copy(
        src_ref=other_map,
        dst_ref=own_map.at[1 - par],
        send_sem=s1,
        recv_sem=r1,
        device_id={"sp": partner},
        device_id_type=MESH,
    ).wait_recv()
    a, b = compose(own_map[0], own_map[1, 0:HD], own_map[1, HD : 2 * HD])
    pair_map[0:HD] = a
    pair_map[HD : 2 * HD] = b

    def row_copies(c, target, slot):
        return [
            pltpu.make_async_remote_copy(
                src_ref=pair_map.at[pl.ds(start, size)],
                dst_ref=row_map.at[slot, pl.ds(place, size)],
                send_sem=s2.at[c, i],
                recv_sem=r2.at[slot, i],
                device_id={"sp": target},
                device_id_type=MESH,
            )
            for i, (start, place, size) in enumerate(((0, 0, HD), (HD + 64 * c, HD, 64)))
        ]

    for c in range(2):
        target = z * NY + rx_y(s, c)

        @pl.when(target != sp)
        def _():
            for copy in row_copies(c, target, pair):
                copy.start()

    for i in range(8, 11):
        loads[i].wait()
    u = ups[...]
    u_raw = lax.dot_general(u, w_all, NN, preferred_element_type=F32).astype(BF16).astype(F32)
    q_raw = lax.dot_general(u, wqs[...], NN, preferred_element_type=F32).astype(BF16).astype(F32)
    u_pre = lax.dot_general(u, wfu, NT, preferred_element_type=F32)
    lane = iota(u_pre.shape, 1)
    u_decay = jnp.sum(jnp.where(lane == head, u_pre, 0.0), axis=1, keepdims=True)
    u_strength = jnp.sum(jnp.where(lane == heads + head, u_pre, 0.0), axis=1, keepdims=True)
    u_act = silu(u_raw)
    new_k, new_v = unit_rows(u_act[:, :HD]), u_act[:, HD:]
    query = unit_rows(silu(q_raw)) * HD ** (-0.5)
    uq[...] = query
    uk[...] = new_k

    @pl.when(is_rx)
    def _():
        row_map[pair, 0:HD] = pair_map[0:HD]
        row_map[pair, HD : HD + 64] = pair_map[pl.ds(HD + 64 * half, 64)]
        for i in range(1, 4):
            for copy in row_copies(0, sp, (pair + i) % 4):
                copy.wait_recv()
        total = row_map[0]
        for i in range(1, 4):
            a, b = compose(total, row_map[i, 0:HD], row_map[i, HD : HD + 64])
            total = jnp.concatenate([a, b], axis=0)
        row_sum[...] = total

        def col_copy(first, size, slot):
            return pltpu.make_async_remote_copy(
                src_ref=row_sum.at[pl.ds(first, size)],
                dst_ref=col_map.at[slot, pl.ds(first, size)],
                send_sem=s3,
                recv_sem=r3.at[slot],
                device_id={"sp": 2 * NY + y},
                device_id_type=MESH,
            )

        @pl.when(z == 0)
        def _():
            col_copy(HD, 64, 0).start()
            col_copy(HD, 64, 0).wait_send()

        @pl.when((z == 1) | (z == 3))
        def _():
            col_copy(0, HD + 64, z).start()
            col_copy(0, HD + 64, z).wait_send()

        @pl.when(z == 2)
        def _():
            q_row, k_row = uq[pl.ds(s, 1), :], uk[pl.ds(s, 1), :]
            at, lanes = iota((8 * N, HD), 0), iota((8 * N, HD), 1)
            inner = at % 8
            picked = jnp.where((inner < 4) & (lanes == 4 * (at // 8) + inner), 1.0, 0.0)
            picked = jnp.where(inner == 4, q_row, picked)
            picked = jnp.where(inner == 5, k_row, picked)
            col_copy(0, HD + 64, 3).wait_recv()
            late_a, late_b = col_map[3, 0:HD], col_map[3, HD : HD + 64]
            a, b = compose(row_sum[...], late_a, late_b)
            col_copy(HD, 64, 0).wait_recv()
            col_copy(0, HD + 64, 1).wait_recv()
            early = dot3(col_map[0, HD : HD + 64], col_map[1, 0:HD]) + col_map[1, HD : HD + 64]
            state = dot3(early, a) + b
            state = jnp.concatenate([state, state], axis=0)
            state = jnp.where(iota((HD, HD), 0) // 64 == half, state, 0.0)
            out = lax.dot_general(
                picked, state, NT, precision=lax.Precision.HIGHEST, preferred_element_type=F32
            )
            msg[...] = out.reshape(N, 8, HD)
            copies = []
            for i in range(1, N):
                to = (sp + i) % N
                copy = pltpu.make_async_remote_copy(
                    src_ref=msg.at[to],
                    dst_ref=fin.at[s, half],
                    send_sem=s4.at[i],
                    recv_sem=r4.at[s, half],
                    device_id={"sp": to},
                    device_id_type=MESH,
                )
                copy.start()
                copies.append(copy)
            fin[s, half] = msg[sp]
            for copy in copies:
                copy.wait_send()

    swap.wait_send()
    for c in range(2):
        target = z * NY + rx_y(s, c)

        @pl.when(target != sp)
        def _():
            for copy in row_copies(c, target, pair):
                copy.wait_send()

    for seq in range(2):
        for c in range(2):

            @pl.when(2 * NY + rx_y(seq, c) != sp)
            def _():
                pltpu.make_async_remote_copy(
                    src_ref=msg.at[0],
                    dst_ref=fin.at[seq, c],
                    send_sem=s4.at[0],
                    recv_sem=r4.at[seq, c],
                    device_id={"sp": sp},
                    device_id_type=MESH,
                ).wait_recv()

    tiles = [fin[seq, 0] + fin[seq, 1] for seq in range(2)]
    for seq in range(2):
        cache_ref[seq, 0] = tiles[seq][0:4].astype(BF16)
    query_state = jnp.concatenate([tile[4:5] for tile in tiles], axis=0)
    key_state = jnp.concatenate([tile[5:6] for tile in tiles], axis=0)
    rate = -speed * softplus(u_decay)
    match = jnp.sum(query * new_k, axis=-1, keepdims=True) * (ceiling * sigmoid(u_strength))
    mixed = jnp.exp(rate) * (query_state - match * key_state) + match * new_v
    scale = lax.rsqrt(jnp.mean(mixed * mixed, axis=-1, keepdims=True) + EPS)
    read_ref[...] = (mixed * scale * gains[...]).astype(BF16)


def on_device(x, wk, wv, wq, wf, wu, speeds, ceilings, mult, spike, up, gain):
    seqs, span, width = x.shape
    heads = wf.shape[1]
    any_space = pl.BlockSpec(memory_space=pl.ANY)
    smem = pl.BlockSpec(memory_space=pltpu.SMEM)
    vmem = pl.BlockSpec(memory_space=pltpu.VMEM)
    dma = pltpu.SemaphoreType.DMA
    return pl.pallas_call(
        kernel,
        out_shape=(
            jax.ShapeDtypeStruct((seqs, 1, HD // N, HD), BF16),
            jax.ShapeDtypeStruct((seqs, HD), BF16),
        ),
        in_specs=[any_space] * 6 + [smem] * 2 + [any_space] * 4,
        out_specs=(vmem, vmem),
        scratch_shapes=[
            pltpu.VMEM((seqs, span, width), BF16),
            pltpu.VMEM((width, 2 * HD), BF16),
            pltpu.VMEM((width, HD), BF16),
            pltpu.VMEM((heads, width), BF16),
            pltpu.VMEM((heads, width), BF16),
            pltpu.VMEM((seqs, 1, span), F32),
            pltpu.VMEM((seqs, 1, span), F32),
            pltpu.VMEM((seqs, width), BF16),
            pltpu.VMEM((1, HD), F32),
            pltpu.VMEM((2 * heads, span), F32),
            pltpu.VMEM((seqs, HD), F32),
            pltpu.VMEM((seqs, HD), F32),
            pltpu.VMEM((2 * HD, HD), F32),
            pltpu.VMEM((2, 2 * HD, HD), F32),
            pltpu.VMEM((2 * HD, HD), F32),
            pltpu.VMEM((4, HD + 64, HD), F32),
            pltpu.VMEM((HD + 64, HD), F32),
            pltpu.VMEM((4, HD + 64, HD), F32),
            pltpu.VMEM((N, 8, HD), F32),
            pltpu.VMEM((2, 2, 8, HD), F32),
            dma((11,)),
            dma,
            dma,
            dma((2, 2)),
            dma((4, 2)),
            dma,
            dma((4,)),
            dma((N,)),
            dma((2, 2)),
        ],
        compiler_params=pltpu.CompilerParams(collective_id=0, has_side_effects=True),
    )(
        x,
        wk,
        wv,
        wq,
        wf.T,
        wu.T,
        speeds,
        ceilings,
        jnp.swapaxes(mult, 1, 2),
        jnp.swapaxes(spike, 1, 2),
        up,
        gain.reshape(1, -1),
    )


def solution(mesh):
    placed = (
        P("gr", "sp", None),
        P(None, "tp"),
        P(None, "tp"),
        P(None, "tp"),
        P(),
        P(),
        P("tp"),
        P("tp"),
        P("gr", "sp", "tp"),
        P("gr", "sp", "tp"),
        P("gr", None),
        P(),
    )
    return jax.shard_map(
        on_device,
        mesh=mesh,
        in_specs=placed,
        out_specs=(P("gr", "tp", "sp", None), P("gr", "tp")),
        check_vma=False,
    )
```

time: 148 us -> 39.1 us (0.26)
  waiting for transfers between devices: 42 us -> 0 us
  blocking collectives: 41.1 us -> 0 us
  matrix products: 36 us -> 0 us
  Pallas kernels: 0 us -> 34.6 us
  between operations: 16 us -> 1.93 us
  starting transfers between devices: 7.62 us -> 0 us
  other arithmetic: 2.99 us -> 0 us
    dot_general x55 -> x0, matrix products: 36 us -> none  [the longest x15 11.5 us: compose(): return jnp.einsum('shij,shjk->shik', left_map, right_map, precision=HIGH)]
    pallas_call x0 -> x1, Pallas kernels: none -> 34.6 us  [on_device(): pl.pallas_call(kernel, out_shape=(jax.ShapeDtypeStruct((seqs, 1, HD // N,...]
    all_gather x1 -> x0, waiting for transfers between devices: 31.7 us -> none  [carried_in(): pieces = lax.all_gather(subtotal, axis)]
    psum x2 -> x0, blocking collectives: 24.5 us -> none  [by_axis(): x = lax.psum(x, axis)]
    all_gather x1 -> x0, blocking collectives: 16.5 us -> none  [carried_in(): pieces = lax.all_gather(subtotal, axis)]
    all_to_all x1 -> x0, waiting for transfers between devices: 10.3 us -> none  [sum_at_owner(): tiles = lax.all_to_all(split_up(x, dim, size), axis, 0, 0, tiled=True)]
    all_to_all x1 -> x0, starting transfers between devices: 7.58 us -> none  [sum_at_owner(): tiles = lax.all_to_all(split_up(x, dim, size), axis, 0, 0, tiled=True)]
    unnamed x22 -> x2, local copies, waits for them, and re-layouts: 0.76 us -> 2.39 us
  transfers between devices with their start and end apart: 2 -> 0, of which waited for: 2 -> 0; matrix products, arithmetic and copies ran while one was open for 9% -> 0% of each run, Pallas kernels for 0% -> 0%
where the time goes in v1:
time: 39.1 us; the launch traced here: 38.9 us
  Pallas kernels  34.6 us (88%)
  local copies, waits for them, and re-layouts  2.39 us (6%)
  between operations  1.93 us (5%)
    pallas_call x1, Pallas kernels, on_device(): pl.pallas_call(kernel, out_shape=(jax.ShapeDtypeStruct((seqs, 1, HD // N,...  34.6 us
    unnamed x2, local copies, waits for them, and re-layouts  2.39 us

profile of v1, /device:TPU:6, one launch (start us, length us, event | category | flops | bytes accessed | tf_op | source)
XLA Modules:
  0.0 38.9 jit_solution(12833529658745362562)
XLA Ops:
  1.9 34.6 %shard_map.131 = (bf16[2,1,4,128]{3,2,1,0:T(4,128)(2,1)}, bf16[2,128]{1,0:T(2,128)(2,1)}) custom-call(bf16[2,256,2048]{2,1,0:T(8,128)(2,1)} %x_hbm.1, bf16[2048,128]{1,0:T(8,128)(2,1)} %wk_hbm.1, bf16[2048,128]{1,0:T(8,128)(2,1)} %wv_hbm.1, bf16[2048,128]{1,0:T(8,128)(2,1)} %wq_hbm.1, bf16[8,2048]{1,0:T(8,128)(2,1)} %bitcast.5, bf16[8,2048]{1,0:T(8,128)(2,1)} %bitcast.6, ...), custom_call_target="tpu_custom_call" | custom-call | tf_op jit(solution)/shard_map/pallas_call | solution.py:387
  36.5 1.3 %copy.18 = bf16[2,1,4,128]{3,2,1,0:T(4,128)(2,1)} copy(bf16[2,1,4,128]{3,2,1,0:T(4,128)(2,1)} %get-tuple-element.4) | data formatting | bytes 4096
  37.7 1.1 %copy.19 = bf16[2,128]{1,0:T(2,128)(2,1)} copy(bf16[2,128]{1,0:T(2,128)(2,1)} %get-tuple-element.5) | data formatting | bytes 1024

commit v2 on v1

v2 whole, which is shorter than its diff:
```python
import jax
import jax.numpy as jnp
from jax import lax
from jax.experimental import pallas as pl
from jax.experimental.pallas import tpu as pltpu
from jax.sharding import PartitionSpec as P

EPS = 1e-06
F32 = jnp.float32
BF16 = jnp.bfloat16
MESH = pl.DeviceIdType.MESH
NY = 8
NZ = 4
N = NY * NZ
ZR = 3
RX0, RX1 = 5, 2
FIRST = (0, 1, 7, 2, 6, 3, 5, 4)
OUT = pltpu.VMEM
CH = 128
HD = 128
NN = (((1,), (0,)), ((), ()))
NT = (((1,), (1,)), ((), ()))


def dot1(a, b, dims=NN):
    return lax.dot_general(a.astype(BF16), b.astype(BF16), dims, preferred_element_type=F32)


def halves(a):
    high = a.astype(BF16)
    return high, (a - high.astype(F32)).astype(BF16)


def dot3(a, b):
    ah, al = halves(a)
    bh, bl = halves(b)
    left = jnp.concatenate([ah, ah, al], axis=1)
    right = jnp.concatenate([bh, bl, bh], axis=0)
    return lax.dot_general(left, right, NN, preferred_element_type=F32)


def silu(z):
    return z / (1.0 + jnp.exp(-z))


def softplus(z):
    return jnp.maximum(z, 0.0) + jnp.log1p(jnp.exp(-jnp.abs(z)))


def sigmoid(z):
    return 1.0 / (1.0 + jnp.exp(-z))


def unit_rows(z):
    return z * lax.rsqrt(jnp.sum(z * z, axis=-1, keepdims=True) + EPS)


def iota(shape, dim):
    return lax.broadcasted_iota(jnp.int32, shape, dim)


def compose(early, late_a, late_b):
    moved = dot3(early, late_a)
    return moved[:HD], moved[HD:] + late_b


def chunk_map(k, v, c, beta):
    rows, cols = iota((CH, CH), 0), iota((CH, CH), 1)
    c_cols = jnp.broadcast_to(c, (CH, CH))
    c_rows = jnp.transpose(c_cols)
    end = c[:, CH - 1 :]
    match = dot1(k, k, NT)
    power = jnp.where(cols > rows, match * beta * jnp.exp(c_cols - c_rows), 0.0)
    k_t, v_t = jnp.transpose(k), jnp.transpose(v)
    rhs = jnp.concatenate([k_t * (-beta * jnp.exp(c)), v_t * beta], axis=0)
    both = dot1(jnp.concatenate([rhs, power], axis=0), power)
    rhs = rhs - both[: 2 * HD]
    power = both[2 * HD :]
    for _ in range(5):
        both = dot1(jnp.concatenate([rhs, power], axis=0), power)
        rhs = rhs + both[: 2 * HD]
        power = both[2 * HD :]
    rhs = rhs + dot1(rhs, power)
    faded = k * jnp.exp(end - c_rows)
    out = dot3(rhs, faded)
    return out[:HD] + jnp.where(rows == cols, jnp.exp(end), 0.0), out[HD:]


def kernel(
    x_hbm,
    wk_hbm,
    wv_hbm,
    wq_hbm,
    wf_hbm,
    wu_hbm,
    speed_ref,
    ceil_ref,
    mult_hbm,
    spike_hbm,
    up_hbm,
    gain_hbm,
    out_ref,
    xs,
    wkv,
    wqs,
    wfs,
    wus,
    mults,
    spikes,
    ups,
    gains,
    dsc,
    uq,
    uk,
    other_map,
    own_map,
    pair_map,
    row_map,
    row_sum,
    col_map,
    msg,
    fin,
    lsem,
    s1,
    r1,
    s2,
    r2,
    s3,
    r3,
    s4,
    r4,
):
    sp = lax.axis_index("sp")
    tp = lax.axis_index("tp")
    y, z = sp % NY, sp // NY
    core = tp % 2
    par, pair = y % 2, y // 2
    turned = (pair - core + 4) % 4
    s = (par + (turned + 1) // 2) % 2
    other = 1 - s

    def rx_y(seq):
        return (RX0 + (RX1 - RX0) * seq + 2 * core) % NY

    is_rx = y == rx_y(s)
    head = tp % wf_hbm.shape[0]

    pairs = [
        (wk_hbm, wkv.at[:, 0:HD]),
        (wv_hbm, wkv.at[:, HD : 2 * HD]),
        (x_hbm.at[other], xs.at[other]),
        (wf_hbm, wfs),
        (wu_hbm, wus),
        (mult_hbm, mults),
        (spike_hbm, spikes),
        (x_hbm.at[s], xs.at[s]),
        (wq_hbm, wqs),
        (up_hbm, ups),
        (gain_hbm, gains),
    ]
    loads = [pltpu.make_async_copy(a, b, lsem.at[i]) for i, (a, b) in enumerate(pairs)]
    first = 7
    for load in loads[:first]:
        load.start()

    barrier = pltpu.get_barrier_semaphore()

    def greet(device):
        pl.semaphore_signal(barrier, inc=1, device_id={"sp": device}, device_id_type=MESH)

    partner = sp + 1 - 2 * par
    greet(partner)

    @pl.when(is_rx)
    def _():
        for i in range(1, 4):
            there = (pair + i) % 4
            greet(z * NY + 2 * there + (s + ((there - core + 4) % 4 + 1) // 2) % 2)

        @pl.when(z == ZR)
        def _():
            for i in range(NZ):
                if i != ZR:
                    greet(i * NY + y)

    with jax.named_scope("p_load"):
        for load in loads[:first]:
            load.wait()
        for load in loads[first:]:
            load.start()
        speed, ceiling = speed_ref[0], ceil_ref[0]
    w_all = wkv[...]
    wfu = jnp.concatenate([wfs[...].astype(F32), wus[...].astype(F32)], axis=0).astype(BF16)
    heads = wf_hbm.shape[0]

    def seq_map(seq):
        x = xs[seq]
        raw = lax.dot_general(x, w_all, NN, preferred_element_type=F32)
        raw = raw.astype(BF16).astype(F32)
        act = silu(raw)
        k, v = unit_rows(act[:, :HD]), act[:, HD:]
        dsc[...] = lax.dot_general(wfu, x, NT, preferred_element_type=F32)
        decay = dsc[pl.ds(head, 1), :]
        strength = dsc[pl.ds(heads + head, 1), :]
        g = -speed * softplus(decay) * mults[seq] + spikes[seq]
        beta = ceiling * sigmoid(strength)
        g_high = g.astype(BF16).astype(F32)
        g_rest = g - g_high
        g_mid = g_rest.astype(BF16).astype(F32)
        g_low = g_rest - g_mid
        row = iota((8, CH), 0)
        parts = jnp.zeros((8, CH), F32)
        place = 0
        for i in range(2):
            for part in (g_high, g_mid, g_low):
                parts = jnp.where(row == place, part[:, i * CH : (i + 1) * CH], parts)
                place += 1
        upper = jnp.where(iota((CH, CH), 0) <= iota((CH, CH), 1), 1.0, 0.0)
        sums = dot1(parts, upper)
        maps = []
        for i in range(2):
            c = sums[3 * i : 3 * i + 1] + sums[3 * i + 1 : 3 * i + 2] + sums[3 * i + 2 : 3 * i + 3]
            sl = slice(i * CH, (i + 1) * CH)
            maps.append(chunk_map(k[sl], v[sl], c, beta[:, sl]))
        early = jnp.concatenate(maps[0], axis=0)
        return compose(early, maps[1][0], maps[1][1])

    with jax.named_scope("p_seqA"):
        a, b = seq_map(other)
        other_map[0:HD] = a
        other_map[HD : 2 * HD] = b
    with jax.named_scope("p_barrier"):
        pl.semaphore_wait(barrier, jnp.where(is_rx & (z == ZR), 1, 2))
    swap = pltpu.make_async_remote_copy(
        src_ref=other_map,
        dst_ref=own_map.at[par],
        send_sem=s1,
        recv_sem=r1,
        device_id={"sp": partner},
        device_id_type=MESH,
    )
    swap.start()
    with jax.named_scope("p_seqB"):
        loads[first].wait()
        a, b = seq_map(s)
        own_map[par, 0:HD] = a
        own_map[par, HD : 2 * HD] = b
    with jax.named_scope("p_r1wait"):
        pltpu.make_async_remote_copy(
            src_ref=other_map,
            dst_ref=own_map.at[1 - par],
            send_sem=s1,
            recv_sem=r1,
            device_id={"sp": partner},
            device_id_type=MESH,
        ).wait_recv()
    with jax.named_scope("p_pair"):
        a, b = compose(own_map[0], own_map[1, 0:HD], own_map[1, HD : 2 * HD])
        pair_map[0:HD] = a
        pair_map[HD : 2 * HD] = b
    def row_copy(slot):
        return pltpu.make_async_remote_copy(
            src_ref=pair_map,
            dst_ref=row_map.at[slot],
            send_sem=s2,
            recv_sem=r2.at[slot],
            device_id={"sp": z * NY + rx_y(s)},
            device_id_type=MESH,
        )

    @pl.when(jnp.logical_not(is_rx))
    def _():
        row_copy(pair).start()

    with jax.named_scope("p_up"):
        for load in loads[first + 1 :]:
            load.wait()
        u = ups[...]
        u_raw = lax.dot_general(u, w_all, NN, preferred_element_type=F32).astype(BF16).astype(F32)
        q_raw = lax.dot_general(u, wqs[...], NN, preferred_element_type=F32).astype(BF16).astype(F32)
        u_pre = lax.dot_general(u, wfu, NT, preferred_element_type=F32)
        lane = iota(u_pre.shape, 1)
        u_decay = jnp.sum(jnp.where(lane == head, u_pre, 0.0), axis=1, keepdims=True)
        u_strength = jnp.sum(jnp.where(lane == heads + head, u_pre, 0.0), axis=1, keepdims=True)
        u_act = silu(u_raw)
        new_k, new_v = unit_rows(u_act[:, :HD]), u_act[:, HD:]
        query = unit_rows(silu(q_raw)) * HD ** (-0.5)
        uq[...] = query
        uk[...] = new_k
    @pl.when(is_rx)
    def _():
        row_map[pair] = pair_map[...]
        with jax.named_scope("p_r2wait"):
            for i in range(1, 4):
                row_copy((pair + i) % 4).wait_recv()
        with jax.named_scope("p_rowsum"):
            a, b = compose(row_map[2], row_map[3, 0:HD], row_map[3, HD:])
            c, d = compose(row_map[0], row_map[1, 0:HD], row_map[1, HD:])
            a, b = compose(jnp.concatenate([c, d], axis=0), a, b)
            row_sum[0:HD] = a
            row_sum[HD:] = b

        def col_copy(first, size, slot):
            return pltpu.make_async_remote_copy(
                src_ref=row_sum.at[pl.ds(first, size)],
                dst_ref=col_map.at[slot, pl.ds(first, size)],
                send_sem=s3,
                recv_sem=r3.at[slot],
                device_id={"sp": ZR * NY + y},
                device_id_type=MESH,
            )

        @pl.when(z == 0)
        def _():
            col_copy(HD, HD, 0).start()
            col_copy(HD, HD, 0).wait_send()

        @pl.when((z != 0) & (z != ZR))
        def _():
            col_copy(0, 2 * HD, z).start()
            col_copy(0, 2 * HD, z).wait_send()

        @pl.when(z == ZR)
        def _():
            q_row, k_row = uq[pl.ds(s, 1), :], uk[pl.ds(s, 1), :]
            at, lanes = iota((8 * N, HD), 0), iota((8 * N, HD), 1)
            inner = at % 8
            picked = jnp.where((inner < 4) & (lanes == 4 * (at // 8) + inner), 1.0, 0.0)
            picked = jnp.where(inner == 4, q_row, picked)
            picked = jnp.where(inner == 5, k_row, picked)
            col_map[ZR] = row_sum[...]
            with jax.named_scope("p_r3wait01"):
                col_copy(HD, HD, 0).wait_recv()
                col_copy(0, 2 * HD, 1).wait_recv()
            with jax.named_scope("p_state1"):
                state = dot3(col_map[0, HD:], col_map[1, 0:HD]) + col_map[1, HD:]
            with jax.named_scope("p_r3wait3"):
                col_copy(0, 2 * HD, 5 - ZR).wait_recv()
            with jax.named_scope("p_state"):
                for i in (2, 3):
                    state = dot3(state, col_map[i, 0:HD]) + col_map[i, HD:]
                out = lax.dot_general(
                    picked, state, NT, precision=lax.Precision.HIGHEST, preferred_element_type=F32
                )
                msg[...] = out.reshape(N, 8, HD)
            def send(to):
                return pltpu.make_async_remote_copy(
                    src_ref=msg.at[to],
                    dst_ref=fin.at[s],
                    send_sem=s4.at[to],
                    recv_sem=r4.at[s],
                    device_id={"sp": to},
                    device_id_type=MESH,
                )

            with jax.named_scope("p_r4send"):
                targets = [i * NY + j for i in range(NZ) for j in FIRST]
                for to in targets:
                    if to // NY == ZR:
                        pl.when(to != sp)(send(to).start)
                    else:
                        send(to).start()
                fin[s] = msg[sp]
            for to in targets:
                if to // NY == ZR:
                    pl.when(to != sp)(send(to).wait_send)
                else:
                    send(to).wait_send()

    swap.wait_send()

    @pl.when(jnp.logical_not(is_rx))
    def _():
        row_copy(pair).wait_send()

    with jax.named_scope("p_r4wait"):
        for seq in range(2):

            @pl.when(ZR * NY + rx_y(seq) != sp)
            def _():
                pltpu.make_async_remote_copy(
                    src_ref=msg.at[0],
                    dst_ref=fin.at[seq],
                    send_sem=s4.at[0],
                    recv_sem=r4.at[seq],
                    device_id={"sp": sp},
                    device_id_type=MESH,
                ).wait_recv()

    with jax.named_scope("p_finish"):
        tiles = [fin[seq] for seq in range(2)]
        query_state = jnp.concatenate([tile[4:5] for tile in tiles], axis=0)
        key_state = jnp.concatenate([tile[5:6] for tile in tiles], axis=0)
        rate = -speed * softplus(u_decay)
        match = jnp.sum(query * new_k, axis=-1, keepdims=True) * (ceiling * sigmoid(u_strength))
        mixed = jnp.exp(rate) * (query_state - match * key_state) + match * new_v
        scale = lax.rsqrt(jnp.mean(mixed * mixed, axis=-1, keepdims=True) + EPS)
        read = mixed * scale * gains[...]
        row = iota((8, HD), 0)
        for seq in range(2):
            out_ref[seq] = jnp.where(row == 4, read[seq : seq + 1], tiles[seq])


def place_outputs(tiles_ref, cache_ref, read_ref):
    for seq in range(2):
        cache_ref[seq, 0] = tiles_ref[seq, 0:4].astype(BF16)
    rows = [tiles_ref[seq, 4:5] for seq in range(2)]
    read_ref[...] = jnp.concatenate(rows, axis=0).astype(BF16)


def on_device(x, wk, wv, wq, wf, wu, speeds, ceilings, mult, spike, up, gain):
    seqs, span, width = x.shape
    heads = wf.shape[1]
    any_space = pl.BlockSpec(memory_space=pl.ANY)
    smem = pl.BlockSpec(memory_space=pltpu.SMEM)
    vmem = pl.BlockSpec(memory_space=pltpu.VMEM)
    dma = pltpu.SemaphoreType.DMA
    out = pl.pallas_call(
        kernel,
        out_shape=OUT((seqs, 8, HD), F32),
        in_specs=[any_space] * 6 + [smem] * 2 + [any_space] * 4,
        out_specs=vmem,
        scratch_shapes=[
            pltpu.VMEM((seqs, span, width), BF16),
            pltpu.VMEM((width, 2 * HD), BF16),
            pltpu.VMEM((width, HD), BF16),
            pltpu.VMEM((heads, width), BF16),
            pltpu.VMEM((heads, width), BF16),
            pltpu.VMEM((seqs, 1, span), F32),
            pltpu.VMEM((seqs, 1, span), F32),
            pltpu.VMEM((seqs, width), BF16),
            pltpu.VMEM((1, HD), F32),
            pltpu.VMEM((2 * heads, span), F32),
            pltpu.VMEM((seqs, HD), F32),
            pltpu.VMEM((seqs, HD), F32),
            pltpu.VMEM((2 * HD, HD), F32),
            pltpu.VMEM((2, 2 * HD, HD), F32),
            pltpu.VMEM((2 * HD, HD), F32),
            pltpu.VMEM((4, 2 * HD, HD), F32),
            pltpu.VMEM((2 * HD, HD), F32),
            pltpu.VMEM((4, 2 * HD, HD), F32),
            pltpu.VMEM((N, 8, HD), F32),
            pltpu.VMEM((2, 8, HD), F32),
            dma((11,)),
            dma,
            dma,
            dma,
            dma((4,)),
            dma,
            dma((4,)),
            dma((N,)),
            dma((2,)),
        ],
        compiler_params=pltpu.CompilerParams(collective_id=0, has_side_effects=True),
    )(
        x,
        wk,
        wv,
        wq,
        wf.T,
        wu.T,
        speeds,
        ceilings,
        jnp.swapaxes(mult, 1, 2),
        jnp.swapaxes(spike, 1, 2),
        up,
        gain.reshape(1, -1),
    )
    return pl.pallas_call(
        place_outputs,
        out_shape=(
            jax.ShapeDtypeStruct((seqs, 1, HD // N, HD), BF16),
            jax.ShapeDtypeStruct((seqs, HD), BF16),
        ),
        in_specs=[vmem],
        out_specs=(vmem, vmem),
    )(pltpu.with_memory_space_constraint(out, pltpu.VMEM))


def solution(mesh):
    placed = (
        P("gr", "sp", None),
        P(None, "tp"),
        P(None, "tp"),
        P(None, "tp"),
        P(),
        P(),
        P("tp"),
        P("tp"),
        P("gr", "sp", "tp"),
        P("gr", "sp", "tp"),
        P("gr", None),
        P(),
    )
    return jax.shard_map(
        on_device,
        mesh=mesh,
        in_specs=placed,
        out_specs=(P("gr", "tp", "sp", None), P("gr", "tp")),
        check_vma=False,
    )
```

time: 39.1 us -> 36.1 us (0.923)
  local copies, waits for them, and re-layouts: 2.39 us -> 0 us
  Pallas kernels: 34.6 us -> 33.6 us
    unnamed x2 -> x0, local copies, waits for them, and re-layouts: 2.39 us -> none
    pallas_call x1 -> x2, Pallas kernels: 34.6 us -> 33.6 us  [the longest x1 33.1 us: on_device(): pl.pallas_call(kernel, out_shape=OUT((seqs, 8, HD), F32), in_specs=[any_s...]
where the time goes in v2:
time: 36.1 us; the launch traced here: 35.6 us
  Pallas kernels  33.6 us (93%)
  between operations  1.93 us (5%)
    pallas_call x1, Pallas kernels, on_device(): pl.pallas_call(kernel, out_shape=OUT((seqs, 8, HD), F32), in_specs=[any_s...  33.1 us

profile of v2, /device:TPU:6, one launch (start us, length us, event | category | flops | bytes accessed | tf_op | source)
XLA Modules:
  0.0 35.6 jit_solution(17442081530202662676)
XLA Ops:
  1.9 33.1 %shard_map.131.tiles_ref = f32[2,8,128]{2,1,0:T(8,128)S(1)} custom-call(bf16[2,256,2048]{2,1,0:T(8,128)(2,1)} %x_hbm.1, bf16[2048,128]{1,0:T(8,128)(2,1)} %wk_hbm.1, bf16[2048,128]{1,0:T(8,128)(2,1)} %wv_hbm.1, bf16[2048,128]{1,0:T(8,128)(2,1)} %wq_hbm.1, bf16[8,2048]{1,0:T(8,128)(2,1)} %bitcast.5, bf16[8,2048]{1,0:T(8,128)(2,1)} %bitcast.6, ...), custom_call_target="tpu_custom_call" | custom-call | tf_op jit(solution)/shard_map/pallas_call | solution.py:418
  35.0 0.6 %shard_map.132 = (bf16[2,1,4,128]{3,2,1,0:T(4,128)(2,1)}, bf16[2,128]{1,0:T(2,128)(2,1)}) custom-call(f32[2,8,128]{2,1,0:T(8,128)S(1)} %shard_map.131.tiles_ref), custom_call_target="tpu_custom_call" | custom-call | tf_op jit(solution)/shard_map/pallas_call | solution.py:469

commit v3 on v2

--- a/solution.py
+++ b/solution.py
@@ -13,6 +13,8 @@
 NZ = 4
 N = NY * NZ
 ZR = 3
+NK = 4
+EARLY = 0
 RX0, RX1 = 5, 2
 FIRST = (0, 1, 7, 2, 6, 3, 5, 4)
 OUT = pltpu.VMEM
@@ -64,26 +66,32 @@
     return moved[:HD], moved[HD:] + late_b
 
 
-def chunk_map(k, v, c, beta):
+def chunk_maps(keys, values, sums, betas):
+    some = range(len(keys))
     rows, cols = iota((CH, CH), 0), iota((CH, CH), 1)
-    c_cols = jnp.broadcast_to(c, (CH, CH))
-    c_rows = jnp.transpose(c_cols)
-    end = c[:, CH - 1 :]
-    match = dot1(k, k, NT)
-    power = jnp.where(cols > rows, match * beta * jnp.exp(c_cols - c_rows), 0.0)
-    k_t, v_t = jnp.transpose(k), jnp.transpose(v)
-    rhs = jnp.concatenate([k_t * (-beta * jnp.exp(c)), v_t * beta], axis=0)
-    both = dot1(jnp.concatenate([rhs, power], axis=0), power)
-    rhs = rhs - both[: 2 * HD]
-    power = both[2 * HD :]
-    for _ in range(5):
-        both = dot1(jnp.concatenate([rhs, power], axis=0), power)
-        rhs = rhs + both[: 2 * HD]
-        power = both[2 * HD :]
-    rhs = rhs + dot1(rhs, power)
-    faded = k * jnp.exp(end - c_rows)
-    out = dot3(rhs, faded)
-    return out[:HD] + jnp.where(rows == cols, jnp.exp(end), 0.0), out[HD:]
+    c_rows = [jnp.transpose(jnp.broadcast_to(c, (CH, CH))) for c in sums]
+    ends = [c[:, CH - 1 :] for c in sums]
+    match = [dot1(k, k, NT) for k in keys]
+    k_t = [jnp.transpose(k) for k in keys]
+    v_t = [jnp.transpose(v) for v in values]
+    power = [
+        jnp.where(cols > rows, match[i] * betas[i] * jnp.exp(sums[i] - c_rows[i]), 0.0)
+        for i in some
+    ]
+    rhs = [
+        jnp.concatenate([k_t[i] * (-betas[i] * jnp.exp(sums[i])), v_t[i] * betas[i]], axis=0)
+        for i in some
+    ]
+    for level in range(6):
+        both = [dot1(jnp.concatenate([power[i], rhs[i]], axis=0), power[i]) for i in some]
+        power = [both[i][:CH] for i in some]
+        applied = [both[i][CH:] for i in some]
+        rhs = [rhs[i] - applied[i] if level == 0 else rhs[i] + applied[i] for i in some]
+    rhs = [rhs[i] + dot1(rhs[i], power[i]) for i in some]
+    faded = [keys[i] * jnp.exp(ends[i] - c_rows[i]) for i in some]
+    out = [dot3(rhs[i], faded[i]) for i in some]
+    decayed = [jnp.where(rows == cols, jnp.exp(ends[i]), 0.0) for i in some]
+    return [(out[i][:HD] + decayed[i], out[i][HD:]) for i in some]
 
 
 def kernel(
@@ -129,28 +137,38 @@
     r3,
     s4,
     r4,
+    row_ready,
+    col_ready,
 ):
     sp = lax.axis_index("sp")
     tp = lax.axis_index("tp")
-    y, z = sp % NY, sp // NY
-    core = tp % 2
-    par, pair = y % 2, y // 2
-    turned = (pair - core + 4) % 4
-    s = (par + (turned + 1) // 2) % 2
+    y, z = lax.rem(sp, NY), lax.div(sp, NY)
+    core = lax.rem(tp, 2)
+    par, pair = lax.rem(y, 2), lax.div(y, 2)
+
+    def offset(there):
+        return lax.div(lax.rem(there - core + 4, 4) + 1, 2)
+
+    s = lax.rem(par + offset(pair), 2)
     other = 1 - s
 
     def rx_y(seq):
-        return (RX0 + (RX1 - RX0) * seq + 2 * core) % NY
+        return lax.rem(RX0 + (RX1 - RX0) * seq + 2 * core, NY)
 
     is_rx = y == rx_y(s)
-    head = tp % wf_hbm.shape[0]
-
-    pairs = [
-        (wk_hbm, wkv.at[:, 0:HD]),
-        (wv_hbm, wkv.at[:, HD : 2 * HD]),
-        (x_hbm.at[other], xs.at[other]),
-        (wf_hbm, wfs),
-        (wu_hbm, wus),
+    heads = wf_hbm.shape[0]
+    head = lax.rem(tp, heads)
+
+    depth = wk_hbm.shape[0] // NK
+    pieces = [pl.ds(i * depth, depth) for i in range(NK)]
+    pairs = [(wf_hbm, wfs), (wu_hbm, wus)]
+    for piece in pieces:
+        pairs += [
+            (wk_hbm.at[piece], wkv.at[piece, 0:HD]),
+            (wv_hbm.at[piece], wkv.at[piece, HD : 2 * HD]),
+            (x_hbm.at[other, :, piece], xs.at[other, :, piece]),
+        ]
+    pairs += [
         (mult_hbm, mults),
         (spike_hbm, spikes),
         (x_hbm.at[s], xs.at[s]),
@@ -159,7 +177,7 @@
         (gain_hbm, gains),
     ]
     loads = [pltpu.make_async_copy(a, b, lsem.at[i]) for i, (a, b) in enumerate(pairs)]
-    first = 7
+    first = 3 * NK + 4
     for load in loads[:first]:
         load.start()
 
@@ -171,35 +189,37 @@
     partner = sp + 1 - 2 * par
     greet(partner)
 
+    def senders(signal):
+        for i in range(1, 4):
+            there = lax.rem(pair + i, 4)
+            signal(z * NY + 2 * there + lax.rem(s + offset(there), 2))
+
     @pl.when(is_rx)
     def _():
-        for i in range(1, 4):
-            there = (pair + i) % 4
-            greet(z * NY + 2 * there + (s + ((there - core + 4) % 4 + 1) // 2) % 2)
-
-        @pl.when(z == ZR)
+        @pl.when(z != ZR)
         def _():
-            for i in range(NZ):
-                if i != ZR:
-                    greet(i * NY + y)
-
-    with jax.named_scope("p_load"):
-        for load in loads[:first]:
-            load.wait()
-        for load in loads[first:]:
-            load.start()
-        speed, ceiling = speed_ref[0], ceil_ref[0]
-    w_all = wkv[...]
+            greet(ZR * NY + y)
+
+    @pl.when(jnp.logical_not(is_rx))
+    def _():
+        greet(z * NY + rx_y(s))
+
+    speed, ceiling = speed_ref[0], ceil_ref[0]
+    loads[0].wait()
+    loads[1].wait()
     wfu = jnp.concatenate([wfs[...].astype(F32), wus[...].astype(F32)], axis=0).astype(BF16)
-    heads = wf_hbm.shape[0]
-
-    def seq_map(seq):
-        x = xs[seq]
-        raw = lax.dot_general(x, w_all, NN, preferred_element_type=F32)
+
+    def project(seq, piece):
+        x = xs[seq, :, piece]
+        raw = lax.dot_general(x, wkv[piece], NN, preferred_element_type=F32)
+        pre = lax.dot_general(wfu[:, piece], x, NT, preferred_element_type=F32)
+        return raw, pre
+
+    def seq_map(seq, raw, pre):
+        dsc[...] = pre
         raw = raw.astype(BF16).astype(F32)
         act = silu(raw)
         k, v = unit_rows(act[:, :HD]), act[:, HD:]
-        dsc[...] = lax.dot_general(wfu, x, NT, preferred_element_type=F32)
         decay = dsc[pl.ds(head, 1), :]
         strength = dsc[pl.ds(heads + head, 1), :]
         g = -speed * softplus(decay) * mults[seq] + spikes[seq]
@@ -217,20 +237,52 @@
                 place += 1
         upper = jnp.where(iota((CH, CH), 0) <= iota((CH, CH), 1), 1.0, 0.0)
         sums = dot1(parts, upper)
-        maps = []
-        for i in range(2):
-            c = sums[3 * i : 3 * i + 1] + sums[3 * i + 1 : 3 * i + 2] + sums[3 * i + 2 : 3 * i + 3]
-            sl = slice(i * CH, (i + 1) * CH)
-            maps.append(chunk_map(k[sl], v[sl], c, beta[:, sl]))
+        slices = [slice(i * CH, (i + 1) * CH) for i in range(2)]
+        maps = chunk_maps(
+            [k[sl] for sl in slices],
+            [v[sl] for sl in slices],
+            [sums[3 * i : 3 * i + 1] + sums[3 * i + 1 : 3 * i + 2] + sums[3 * i + 2 : 3 * i + 3] for i in range(2)],
+            [beta[:, sl] for sl in slices],
+        )
         early = jnp.concatenate(maps[0], axis=0)
         return compose(early, maps[1][0], maps[1][1])
 
     with jax.named_scope("p_seqA"):
-        a, b = seq_map(other)
+        raw, pre = None, None
+        for i in range(NK):
+            for load in loads[2 + 3 * i : 5 + 3 * i]:
+                load.wait()
+            if i == NK - 2:
+                loads[first].start()
+            raw_part, pre_part = project(other, slice(i * depth, (i + 1) * depth))
+            raw = raw_part if raw is None else raw + raw_part
+            pre = pre_part if pre is None else pre + pre_part
+        for load in loads[first + 1 :]:
+            load.start()
+        for load in loads[first - 2 : first]:
+            load.wait()
+        a, b = seq_map(other, raw, pre)
         other_map[0:HD] = a
         other_map[HD : 2 * HD] = b
     with jax.named_scope("p_barrier"):
-        pl.semaphore_wait(barrier, jnp.where(is_rx & (z == ZR), 1, 2))
+        expected = jnp.where(is_rx, jnp.where(z == ZR, 4 + NZ - 1, 4), 1)
+        pl.semaphore_wait(barrier, expected)
+
+    @pl.when(is_rx)
+    def _():
+        def ready(device):
+            pl.semaphore_signal(row_ready, inc=1, device_id={"sp": device}, device_id_type=MESH)
+
+        senders(ready)
+
+        @pl.when(z == ZR)
+        def _():
+            for i in range(NZ):
+                if i != ZR:
+                    pl.semaphore_signal(
+                        col_ready, inc=1, device_id={"sp": i * NY + y}, device_id_type=MESH
+                    )
+
     swap = pltpu.make_async_remote_copy(
         src_ref=other_map,
         dst_ref=own_map.at[par],
@@ -239,12 +291,14 @@
         device_id={"sp": partner},
         device_id_type=MESH,
     )
-    swap.start()
+    early = core == EARLY
+    pl.when(early)(swap.start)
     with jax.named_scope("p_seqB"):
         loads[first].wait()
-        a, b = seq_map(s)
+        a, b = seq_map(s, *project(s, slice(0, NK * depth)))
         own_map[par, 0:HD] = a
         own_map[par, HD : 2 * HD] = b
+    pl.when(jnp.logical_not(early))(swap.start)
     with jax.named_scope("p_r1wait"):
         pltpu.make_async_remote_copy(
             src_ref=other_map,
@@ -270,11 +324,13 @@
 
     @pl.when(jnp.logical_not(is_rx))
     def _():
+        pl.semaphore_wait(row_ready, 1)
         row_copy(pair).start()
 
     with jax.named_scope("p_up"):
         for load in loads[first + 1 :]:
             load.wait()
+        w_all = wkv[...]
         u = ups[...]
         u_raw = lax.dot_general(u, w_all, NN, preferred_element_type=F32).astype(BF16).astype(F32)
         q_raw = lax.dot_general(u, wqs[...], NN, preferred_element_type=F32).astype(BF16).astype(F32)
@@ -292,7 +348,7 @@
         row_map[pair] = pair_map[...]
         with jax.named_scope("p_r2wait"):
             for i in range(1, 4):
-                row_copy((pair + i) % 4).wait_recv()
+                row_copy(lax.rem(pair + i, 4)).wait_recv()
         with jax.named_scope("p_rowsum"):
             a, b = compose(row_map[2], row_map[3, 0:HD], row_map[3, HD:])
             c, d = compose(row_map[0], row_map[1, 0:HD], row_map[1, HD:])
@@ -312,11 +368,13 @@
 
         @pl.when(z == 0)
         def _():
+            pl.semaphore_wait(col_ready, 1)
             col_copy(HD, HD, 0).start()
             col_copy(HD, HD, 0).wait_send()
 
         @pl.when((z != 0) & (z != ZR))
         def _():
+            pl.semaphore_wait(col_ready, 1)
             col_copy(0, 2 * HD, z).start()
             col_copy(0, 2 * HD, z).wait_send()
 
@@ -399,6 +457,10 @@
         row = iota((8, HD), 0)
         for seq in range(2):
             out_ref[seq] = jnp.where(row == 4, read[seq : seq + 1], tiles[seq])
+
+
+def near(a):
+    return pltpu.with_memory_space_constraint(a, pltpu.VMEM)
 
 
 def place_outputs(tiles_ref, cache_ref, read_ref):
@@ -441,7 +503,7 @@
             pltpu.VMEM((4, 2 * HD, HD), F32),
             pltpu.VMEM((N, 8, HD), F32),
             pltpu.VMEM((2, 8, HD), F32),
-            dma((11,)),
+            dma((3 * NK + 8,)),
             dma,
             dma,
             dma,
@@ -450,6 +512,8 @@
             dma((4,)),
             dma((N,)),
             dma((2,)),
+            pltpu.SemaphoreType.REGULAR,
+            pltpu.SemaphoreType.REGULAR,
         ],
         compiler_params=pltpu.CompilerParams(collective_id=0, has_side_effects=True),
     )(
@@ -474,7 +538,7 @@
         ),
         in_specs=[vmem],
         out_specs=(vmem, vmem),
-    )(pltpu.with_memory_space_constraint(out, pltpu.VMEM))
+    )(near(out))
 
 
 def solution(mesh):

time: 36.1 us -> 34.9 us (0.967)
  the two profiles are of different devices: /device:TPU:6 before, /device:TPU:8 now
where the time goes in v3:
time: 34.9 us; the launch traced here: 34.7 us
  Pallas kernels  32.8 us (94%)
  between operations  1.93 us (6%)
    pallas_call x1, Pallas kernels, on_device(): pl.pallas_call(kernel, out_shape=OUT((seqs, 8, HD), F32), in_specs=[any_s...  32.2 us

profile of v3, /device:TPU:8, one launch (start us, length us, event | category | flops | bytes accessed | tf_op | source)
XLA Modules:
  0.0 34.7 jit_solution(26472379432770159)
XLA Ops:
  1.9 32.2 %shard_map.131.tiles_ref = f32[2,8,128]{2,1,0:T(8,128)S(1)} custom-call(bf16[2,256,2048]{2,1,0:T(8,128)(2,1)} %x_hbm.1, bf16[2048,128]{1,0:T(8,128)(2,1)} %wk_hbm.1, bf16[2048,128]{1,0:T(8,128)(2,1)} %wv_hbm.1, bf16[2048,128]{1,0:T(8,128)(2,1)} %wq_hbm.1, bf16[8,2048]{1,0:T(8,128)(2,1)} %bitcast.5, bf16[8,2048]{1,0:T(8,128)(2,1)} %bitcast.6, ...), custom_call_target="tpu_custom_call" | custom-call | tf_op jit(solution)/shard_map/pallas_call | solution.py:480
  34.1 0.6 %shard_map.132 = (bf16[2,1,4,128]{3,2,1,0:T(4,128)(2,1)}, bf16[2,128]{1,0:T(2,128)(2,1)}) custom-call(f32[2,8,128]{2,1,0:T(8,128)S(1)} %shard_map.131.tiles_ref), custom_call_target="tpu_custom_call" | custom-call | tf_op jit(solution)/shard_map/pallas_call | solution.py:533

commit v4 on v3

--- a/solution.py
+++ b/solution.py
@@ -15,7 +15,7 @@
 ZR = 3
 NK = 4
 EARLY = 0
-RX0, RX1 = 5, 2
+RX0, RX1 = 6, 2
 FIRST = (0, 1, 7, 2, 6, 3, 5, 4)
 OUT = pltpu.VMEM
 CH = 128
@@ -33,12 +33,12 @@
     return high, (a - high.astype(F32)).astype(BF16)
 
 
-def dot3(a, b):
+def dot3(a, b, dims=NN):
     ah, al = halves(a)
     bh, bl = halves(b)
     left = jnp.concatenate([ah, ah, al], axis=1)
-    right = jnp.concatenate([bh, bl, bh], axis=0)
-    return lax.dot_general(left, right, NN, preferred_element_type=F32)
+    right = jnp.concatenate([bh, bl, bh], axis=dims[0][1][0])
+    return lax.dot_general(left, right, dims, preferred_element_type=F32)
 
 
 def silu(z):
@@ -59,11 +59,6 @@
 
 def iota(shape, dim):
     return lax.broadcasted_iota(jnp.int32, shape, dim)
-
-
-def compose(early, late_a, late_b):
-    moved = dot3(early, late_a)
-    return moved[:HD], moved[HD:] + late_b
 
 
 def chunk_maps(keys, values, sums, betas):
@@ -89,9 +84,15 @@
         rhs = [rhs[i] - applied[i] if level == 0 else rhs[i] + applied[i] for i in some]
     rhs = [rhs[i] + dot1(rhs[i], power[i]) for i in some]
     faded = [keys[i] * jnp.exp(ends[i] - c_rows[i]) for i in some]
-    out = [dot3(rhs[i], faded[i]) for i in some]
     decayed = [jnp.where(rows == cols, jnp.exp(ends[i]), 0.0) for i in some]
-    return [(out[i][:HD] + decayed[i], out[i][HD:]) for i in some]
+    turned = [dot3(rhs[i][:HD], faded[i]) + decayed[i] for i in some]
+    whole = dot3(turned[0], turned[1])
+
+    def added():
+        parts = [dot3(rhs[i][HD:], faded[i]) for i in some]
+        return dot3(parts[0], turned[1]) + parts[1]
+
+    return whole, added
 
 
 def kernel(
@@ -238,14 +239,12 @@
         upper = jnp.where(iota((CH, CH), 0) <= iota((CH, CH), 1), 1.0, 0.0)
         sums = dot1(parts, upper)
         slices = [slice(i * CH, (i + 1) * CH) for i in range(2)]
-        maps = chunk_maps(
+        return chunk_maps(
             [k[sl] for sl in slices],
             [v[sl] for sl in slices],
             [sums[3 * i : 3 * i + 1] + sums[3 * i + 1 : 3 * i + 2] + sums[3 * i + 2 : 3 * i + 3] for i in range(2)],
             [beta[:, sl] for sl in slices],
         )
-        early = jnp.concatenate(maps[0], axis=0)
-        return compose(early, maps[1][0], maps[1][1])
 
     with jax.named_scope("p_seqA"):
         raw, pre = None, None
@@ -261,9 +260,9 @@
             load.start()
         for load in loads[first - 2 : first]:
             load.wait()
-        a, b = seq_map(other, raw, pre)
-        other_map[0:HD] = a
-        other_map[HD : 2 * HD] = b
+        whole, added = seq_map(other, raw, pre)
+        other_map[0:HD] = whole
+
     with jax.named_scope("p_barrier"):
         expected = jnp.where(is_rx, jnp.where(z == ZR, 4 + NZ - 1, 4), 1)
         pl.semaphore_wait(barrier, expected)
@@ -283,41 +282,48 @@
                         col_ready, inc=1, device_id={"sp": i * NY + y}, device_id_type=MESH
                     )
 
-    swap = pltpu.make_async_remote_copy(
-        src_ref=other_map,
-        dst_ref=own_map.at[par],
-        send_sem=s1,
-        recv_sem=r1,
-        device_id={"sp": partner},
-        device_id_type=MESH,
-    )
+    def swap(part, slot):
+        rows = pl.ds(part * HD, HD)
+        return pltpu.make_async_remote_copy(
+            src_ref=other_map.at[rows],
+            dst_ref=own_map.at[slot, rows],
+            send_sem=s1.at[part],
+            recv_sem=r1.at[part],
+            device_id={"sp": partner},
+            device_id_type=MESH,
+        )
+
     early = core == EARLY
-    pl.when(early)(swap.start)
+    pl.when(early)(swap(0, par).start)
+    with jax.named_scope("p_seqA2"):
+        other_map[HD : 2 * HD] = added()
+    pl.when(early)(swap(1, par).start)
     with jax.named_scope("p_seqB"):
         loads[first].wait()
-        a, b = seq_map(s, *project(s, slice(0, NK * depth)))
-        own_map[par, 0:HD] = a
-        own_map[par, HD : 2 * HD] = b
-    pl.when(jnp.logical_not(early))(swap.start)
+        raw, pre = project(s, slice(0, NK * depth))
+
+    with jax.named_scope("p_seqB2"):
+        whole, added = seq_map(s, raw, pre)
+        own_map[par, 0:HD] = whole
+        own_map[par, HD : 2 * HD] = added()
+
+    @pl.when(jnp.logical_not(early))
+    def _():
+        swap(0, par).start()
+        swap(1, par).start()
+
     with jax.named_scope("p_r1wait"):
-        pltpu.make_async_remote_copy(
-            src_ref=other_map,
-            dst_ref=own_map.at[1 - par],
-            send_sem=s1,
-            recv_sem=r1,
-            device_id={"sp": partner},
-            device_id_type=MESH,
-        ).wait_recv()
+        swap(0, 1 - par).wait_recv()
     with jax.named_scope("p_pair"):
-        a, b = compose(own_map[0], own_map[1, 0:HD], own_map[1, HD : 2 * HD])
-        pair_map[0:HD] = a
-        pair_map[HD : 2 * HD] = b
-    def row_copy(slot):
+        pair_map[0:HD] = dot3(own_map[0, 0:HD], own_map[1, 0:HD])
+
+    def row_copy(part, slot):
+        rows = pl.ds(part * HD, HD)
         return pltpu.make_async_remote_copy(
-            src_ref=pair_map,
-            dst_ref=row_map.at[slot],
-            send_sem=s2,
-            recv_sem=r2.at[slot],
+            src_ref=pair_map.at[rows],
+            dst_ref=row_map.at[slot, rows],
+            send_sem=s2.at[part],
+            recv_sem=r2.at[slot, part],
             device_id={"sp": z * NY + rx_y(s)},
             device_id_type=MESH,
         )
@@ -325,7 +331,18 @@
     @pl.when(jnp.logical_not(is_rx))
     def _():
         pl.semaphore_wait(row_ready, 1)
-        row_copy(pair).start()
+        row_copy(0, pair).start()
+
+    with jax.named_scope("p_r1wait2"):
+        swap(1, 1 - par).wait_recv()
+    with jax.named_scope("p_pair2"):
+        pair_map[HD : 2 * HD] = (
+            dot3(own_map[0, HD : 2 * HD], own_map[1, 0:HD]) + own_map[1, HD : 2 * HD]
+        )
+
+    @pl.when(jnp.logical_not(is_rx))
+    def _():
+        row_copy(1, pair).start()
 
     with jax.named_scope("p_up"):
         for load in loads[first + 1 :]:
@@ -348,35 +365,50 @@
         row_map[pair] = pair_map[...]
         with jax.named_scope("p_r2wait"):
             for i in range(1, 4):
-                row_copy(lax.rem(pair + i, 4)).wait_recv()
+                row_copy(0, lax.rem(pair + i, 4)).wait_recv()
         with jax.named_scope("p_rowsum"):
-            a, b = compose(row_map[2], row_map[3, 0:HD], row_map[3, HD:])
-            c, d = compose(row_map[0], row_map[1, 0:HD], row_map[1, HD:])
-            a, b = compose(jnp.concatenate([c, d], axis=0), a, b)
-            row_sum[0:HD] = a
-            row_sum[HD:] = b
-
-        def col_copy(first, size, slot):
+            back = dot3(row_map[2, 0:HD], row_map[3, 0:HD])
+            whole = dot3(dot3(row_map[0, 0:HD], row_map[1, 0:HD]), back)
+            row_sum[0:HD] = whole
+
+        def col_copy(part, slot):
+            rows = pl.ds(part * HD, HD)
             return pltpu.make_async_remote_copy(
-                src_ref=row_sum.at[pl.ds(first, size)],
-                dst_ref=col_map.at[slot, pl.ds(first, size)],
-                send_sem=s3,
-                recv_sem=r3.at[slot],
+                src_ref=row_sum.at[rows],
+                dst_ref=col_map.at[slot, rows],
+                send_sem=s3.at[part],
+                recv_sem=r3.at[slot, part],
                 device_id={"sp": ZR * NY + y},
                 device_id_type=MESH,
             )
 
-        @pl.when(z == 0)
+        @pl.when(z != ZR)
         def _():
             pl.semaphore_wait(col_ready, 1)
-            col_copy(HD, HD, 0).start()
-            col_copy(HD, HD, 0).wait_send()
 
         @pl.when((z != 0) & (z != ZR))
         def _():
-            pl.semaphore_wait(col_ready, 1)
-            col_copy(0, 2 * HD, z).start()
-            col_copy(0, 2 * HD, z).wait_send()
+            col_copy(0, z).start()
+
+        with jax.named_scope("p_r2wait2"):
+            for i in range(1, 4):
+                row_copy(1, lax.rem(pair + i, 4)).wait_recv()
+        with jax.named_scope("p_rowsum2"):
+            n01 = dot3(row_map[0, HD:], row_map[1, 0:HD]) + row_map[1, HD:]
+            n23 = dot3(row_map[2, HD:], row_map[3, 0:HD]) + row_map[3, HD:]
+            row_sum[HD:] = dot3(n01, back) + n23
+
+        @pl.when(z != ZR)
+        def _():
+            col_copy(1, z).start()
+
+        @pl.when((z != 0) & (z != ZR))
+        def _():
+            col_copy(0, z).wait_send()
+
+        @pl.when(z != ZR)
+        def _():
+            col_copy(1, z).wait_send()
 
         @pl.when(z == ZR)
         def _():
@@ -386,21 +418,22 @@
             picked = jnp.where((inner < 4) & (lanes == 4 * (at // 8) + inner), 1.0, 0.0)
             picked = jnp.where(inner == 4, q_row, picked)
             picked = jnp.where(inner == 5, k_row, picked)
-            col_map[ZR] = row_sum[...]
+            last_a = dot3(picked, row_sum[0:HD], NT)
+            last_b = dot3(picked, row_sum[HD:], NT)
             with jax.named_scope("p_r3wait01"):
-                col_copy(HD, HD, 0).wait_recv()
-                col_copy(0, 2 * HD, 1).wait_recv()
+                col_copy(1, 0).wait_recv()
+                col_copy(0, 1).wait_recv()
+                col_copy(1, 1).wait_recv()
             with jax.named_scope("p_state1"):
                 state = dot3(col_map[0, HD:], col_map[1, 0:HD]) + col_map[1, HD:]
             with jax.named_scope("p_r3wait3"):
-                col_copy(0, 2 * HD, 5 - ZR).wait_recv()
+                col_copy(0, 2).wait_recv()
+                state = dot3(state, col_map[2, 0:HD])
+                col_copy(1, 2).wait_recv()
             with jax.named_scope("p_state"):
-                for i in (2, 3):
-                    state = dot3(state, col_map[i, 0:HD]) + col_map[i, HD:]
-                out = lax.dot_general(
-                    picked, state, NT, precision=lax.Precision.HIGHEST, preferred_element_type=F32
-                )
-                msg[...] = out.reshape(N, 8, HD)
+                state = state + col_map[2, HD:]
+                msg[...] = (dot3(last_a, state, NT) + last_b).reshape(N, 8, HD)
+
             def send(to):
                 return pltpu.make_async_remote_copy(
                     src_ref=msg.at[to],
@@ -425,11 +458,13 @@
                 else:
                     send(to).wait_send()
 
-    swap.wait_send()
+    for part in range(2):
+        swap(part, par).wait_send()
 
     @pl.when(jnp.logical_not(is_rx))
     def _():
-        row_copy(pair).wait_send()
+        for part in range(2):
+            row_copy(part, pair).wait_send()
 
     with jax.named_scope("p_r4wait"):
         for seq in range(2):
@@ -504,12 +539,12 @@
             pltpu.VMEM((N, 8, HD), F32),
             pltpu.VMEM((2, 8, HD), F32),
             dma((3 * NK + 8,)),
-            dma,
-            dma,
-            dma,
-            dma((4,)),
-            dma,
-            dma((4,)),
+            dma((2,)),
+            dma((2,)),
+            dma((2,)),
+            dma((4, 2)),
+            dma((2,)),
+            dma((4, 2)),
             dma((N,)),
             dma((2,)),
             pltpu.SemaphoreType.REGULAR,

time: 34.9 us -> 33.3 us (0.954)
  the two profiles are of different devices: /device:TPU:8 before, /device:TPU:6 now
where the time goes in v4:
time: 33.3 us; the launch traced here: 33 us
  Pallas kernels  31.1 us (93%)
  between operations  1.93 us (6%)
    pallas_call x1, Pallas kernels, on_device(): pl.pallas_call(kernel, out_shape=OUT((seqs, 8, HD), F32), in_specs=[any_s...  30.5 us

profile of v4, /device:TPU:6, one launch (start us, length us, event | category | flops | bytes accessed | tf_op | source)
XLA Modules:
  0.0 33.0 jit_solution(11689702427056072773)
XLA Ops:
  1.9 30.5 %shard_map.131.tiles_ref = f32[2,8,128]{2,1,0:T(8,128)S(1)} custom-call(bf16[2,256,2048]{2,1,0:T(8,128)(2,1)} %x_hbm.1, bf16[2048,128]{1,0:T(8,128)(2,1)} %wk_hbm.1, bf16[2048,128]{1,0:T(8,128)(2,1)} %wv_hbm.1, bf16[2048,128]{1,0:T(8,128)(2,1)} %wq_hbm.1, bf16[8,2048]{1,0:T(8,128)(2,1)} %bitcast.5, bf16[8,2048]{1,0:T(8,128)(2,1)} %bitcast.6, ...), custom_call_target="tpu_custom_call" | custom-call | tf_op jit(solution)/shard_map/pallas_call | solution.py:515
  32.4 0.6 %shard_map.132 = (bf16[2,1,4,128]{3,2,1,0:T(4,128)(2,1)}, bf16[2,128]{1,0:T(2,128)(2,1)}) custom-call(f32[2,8,128]{2,1,0:T(8,128)S(1)} %shard_map.131.tiles_ref), custom_call_target="tpu_custom_call" | custom-call | tf_op jit(solution)/shard_map/pallas_call | solution.py:568

commit v5 on v4

--- a/solution.py
+++ b/solution.py
@@ -12,11 +12,12 @@
 NY = 8
 NZ = 4
 N = NY * NZ
-ZR = 3
+ZR = 2
 NK = 4
 EARLY = 0
 RX0, RX1 = 6, 2
 FIRST = (0, 1, 7, 2, 6, 3, 5, 4)
+TARGETS = tuple(i * NY + j for i in (0, 1, 3, 2) for j in FIRST)
 OUT = pltpu.VMEM
 CH = 128
 HD = 128
@@ -108,7 +109,8 @@
     spike_hbm,
     up_hbm,
     gain_hbm,
-    out_ref,
+    fin,
+    aux_out,
     xs,
     wkv,
     wqs,
@@ -128,7 +130,7 @@
     row_sum,
     col_map,
     msg,
-    fin,
+    aux,
     lsem,
     s1,
     r1,
@@ -162,25 +164,35 @@
 
     depth = wk_hbm.shape[0] // NK
     pieces = [pl.ds(i * depth, depth) for i in range(NK)]
-    pairs = [(wf_hbm, wfs), (wu_hbm, wus)]
-    for piece in pieces:
+    pairs = [(wf_hbm, wfs, NK), (wu_hbm, wus, NK + 1)]
+    for i, piece in enumerate(pieces):
         pairs += [
-            (wk_hbm.at[piece], wkv.at[piece, 0:HD]),
-            (wv_hbm.at[piece], wkv.at[piece, HD : 2 * HD]),
-            (x_hbm.at[other, :, piece], xs.at[other, :, piece]),
+            (wk_hbm.at[piece], wkv.at[piece, 0:HD], i),
+            (wv_hbm.at[piece], wkv.at[piece, HD : 2 * HD], i),
+            (x_hbm.at[other, :, piece], xs.at[other, :, piece], i),
         ]
     pairs += [
-        (mult_hbm, mults),
-        (spike_hbm, spikes),
-        (x_hbm.at[s], xs.at[s]),
-        (wq_hbm, wqs),
-        (up_hbm, ups),
-        (gain_hbm, gains),
+        (mult_hbm, mults, NK + 2),
+        (spike_hbm, spikes, NK + 3),
+        (x_hbm.at[s], xs.at[s], 0),
+        (wq_hbm, wqs, 1),
+        (up_hbm, ups, 2),
+        (gain_hbm, gains, 3),
     ]
-    loads = [pltpu.make_async_copy(a, b, lsem.at[i]) for i, (a, b) in enumerate(pairs)]
+    loads = [pltpu.make_async_copy(a, b, lsem.at[i]) for a, b, i in pairs]
     first = 3 * NK + 4
     for load in loads[:first]:
         load.start()
+
+    def sent(ref, sem):
+        pltpu.make_async_remote_copy(
+            src_ref=ref,
+            dst_ref=ref,
+            send_sem=sem,
+            recv_sem=r1.at[0],
+            device_id={"sp": sp},
+            device_id_type=MESH,
+        ).wait_send()
 
     barrier = pltpu.get_barrier_semaphore()
 
@@ -249,8 +261,8 @@
     with jax.named_scope("p_seqA"):
         raw, pre = None, None
         for i in range(NK):
-            for load in loads[2 + 3 * i : 5 + 3 * i]:
-                load.wait()
+            piece = xs.at[other, :, pl.ds(0, 2 * depth)]
+            pltpu.make_async_copy(piece, piece, lsem.at[i]).wait()
             if i == NK - 2:
                 loads[first].start()
             raw_part, pre_part = project(other, slice(i * depth, (i + 1) * depth))
@@ -276,18 +288,18 @@
 
         @pl.when(z == ZR)
         def _():
-            for i in range(NZ):
-                if i != ZR:
-                    pl.semaphore_signal(
-                        col_ready, inc=1, device_id={"sp": i * NY + y}, device_id_type=MESH
-                    )
+            for i in range(1, NZ):
+                there = lax.rem(z + i, NZ) * NY + y
+                pl.semaphore_signal(
+                    col_ready, inc=1, device_id={"sp": there}, device_id_type=MESH
+                )
 
     def swap(part, slot):
         rows = pl.ds(part * HD, HD)
         return pltpu.make_async_remote_copy(
             src_ref=other_map.at[rows],
             dst_ref=own_map.at[slot, rows],
-            send_sem=s1.at[part],
+            send_sem=s1,
             recv_sem=r1.at[part],
             device_id={"sp": partner},
             device_id_type=MESH,
@@ -322,7 +334,7 @@
         return pltpu.make_async_remote_copy(
             src_ref=pair_map.at[rows],
             dst_ref=row_map.at[slot, rows],
-            send_sem=s2.at[part],
+            send_sem=s2,
             recv_sem=r2.at[slot, part],
             device_id={"sp": z * NY + rx_y(s)},
             device_id_type=MESH,
@@ -360,6 +372,15 @@
         query = unit_rows(silu(q_raw)) * HD ** (-0.5)
         uq[...] = query
         uk[...] = new_k
+        rate = -speed * softplus(u_decay)
+        match = jnp.sum(query * new_k, axis=-1, keepdims=True) * (ceiling * sigmoid(u_strength))
+        fading = jnp.exp(rate)
+        rows = (fading, fading * match, match * new_v, gains[...])
+        for i, value in enumerate(rows):
+            aux[i] = jnp.broadcast_to(value, (2, HD))
+        aux_copy = pltpu.make_async_copy(aux, aux_out, lsem.at[NK + 1])
+        aux_copy.start()
+
     @pl.when(is_rx)
     def _():
         row_map[pair] = pair_map[...]
@@ -376,19 +397,22 @@
             return pltpu.make_async_remote_copy(
                 src_ref=row_sum.at[rows],
                 dst_ref=col_map.at[slot, rows],
-                send_sem=s3.at[part],
+                send_sem=s3,
                 recv_sem=r3.at[slot, part],
                 device_id={"sp": ZR * NY + y},
                 device_id_type=MESH,
             )
 
+        def run(part, action):
+            @pl.when((z != ZR) & (z >= 1 - part))
+            def _():
+                action(col_copy(part, z))
+
         @pl.when(z != ZR)
         def _():
             pl.semaphore_wait(col_ready, 1)
 
-        @pl.when((z != 0) & (z != ZR))
-        def _():
-            col_copy(0, z).start()
+        run(0, lambda copy: copy.start())
 
         with jax.named_scope("p_r2wait2"):
             for i in range(1, 4):
@@ -398,17 +422,7 @@
             n23 = dot3(row_map[2, HD:], row_map[3, 0:HD]) + row_map[3, HD:]
             row_sum[HD:] = dot3(n01, back) + n23
 
-        @pl.when(z != ZR)
-        def _():
-            col_copy(1, z).start()
-
-        @pl.when((z != 0) & (z != ZR))
-        def _():
-            col_copy(0, z).wait_send()
-
-        @pl.when(z != ZR)
-        def _():
-            col_copy(1, z).wait_send()
+        run(1, lambda copy: copy.start())
 
         @pl.when(z == ZR)
         def _():
@@ -418,53 +432,61 @@
             picked = jnp.where((inner < 4) & (lanes == 4 * (at // 8) + inner), 1.0, 0.0)
             picked = jnp.where(inner == 4, q_row, picked)
             picked = jnp.where(inner == 5, k_row, picked)
-            last_a = dot3(picked, row_sum[0:HD], NT)
-            last_b = dot3(picked, row_sum[HD:], NT)
+
+            def arrive(part, slot):
+                col_copy(part, slot).wait_recv()
+                return col_map[slot, part * HD : (part + 1) * HD]
+
             with jax.named_scope("p_r3wait01"):
-                col_copy(1, 0).wait_recv()
-                col_copy(0, 1).wait_recv()
-                col_copy(1, 1).wait_recv()
+                early_b = arrive(1, 0)
+                late_a = arrive(0, 1)
+                late_b = arrive(1, 1)
             with jax.named_scope("p_state1"):
-                state = dot3(col_map[0, HD:], col_map[1, 0:HD]) + col_map[1, HD:]
+                state = dot3(early_b, late_a) + late_b
+                state = dot3(state, row_sum[0:HD]) + row_sum[HD:]
             with jax.named_scope("p_r3wait3"):
-                col_copy(0, 2).wait_recv()
-                state = dot3(state, col_map[2, 0:HD])
-                col_copy(1, 2).wait_recv()
+                last_a = dot3(picked, arrive(0, 3), NT)
+                late_b = arrive(1, 3)
             with jax.named_scope("p_state"):
-                state = state + col_map[2, HD:]
-                msg[...] = (dot3(last_a, state, NT) + last_b).reshape(N, 8, HD)
+                out = dot3(last_a, state, NT) + dot3(picked, late_b, NT)
+                msg[...] = out.reshape(N, 8, HD)
 
             def send(to):
                 return pltpu.make_async_remote_copy(
                     src_ref=msg.at[to],
                     dst_ref=fin.at[s],
-                    send_sem=s4.at[to],
+                    send_sem=s4,
                     recv_sem=r4.at[s],
                     device_id={"sp": to},
                     device_id_type=MESH,
                 )
 
-            with jax.named_scope("p_r4send"):
-                targets = [i * NY + j for i in range(NZ) for j in FIRST]
-                for to in targets:
+            def each(action):
+                for to in TARGETS:
                     if to // NY == ZR:
-                        pl.when(to != sp)(send(to).start)
+                        pl.when(to != sp)(lambda: action(send(to)))
                     else:
-                        send(to).start()
-                fin[s] = msg[sp]
-            for to in targets:
-                if to // NY == ZR:
-                    pl.when(to != sp)(send(to).wait_send)
-                else:
-                    send(to).wait_send()
-
-    for part in range(2):
-        swap(part, par).wait_send()
+                        action(send(to))
+
+            each(lambda copy: copy.start())
+            own = pltpu.make_async_copy(msg.at[sp], fin.at[s], lsem.at[NK])
+            own.start()
+            own.wait()
+            sent(msg.at[0 : N - 1], s4)
+
+        @pl.when(z == 0)
+        def _():
+            sent(row_sum.at[0:HD], s3)
+
+        @pl.when((z != 0) & (z != ZR))
+        def _():
+            sent(row_sum, s3)
+
+    sent(other_map, s1)
 
     @pl.when(jnp.logical_not(is_rx))
     def _():
-        for part in range(2):
-            row_copy(part, pair).wait_send()
+        sent(pair_map, s2)
 
     with jax.named_scope("p_r4wait"):
         for seq in range(2):
@@ -474,35 +496,28 @@
                 pltpu.make_async_remote_copy(
                     src_ref=msg.at[0],
                     dst_ref=fin.at[seq],
-                    send_sem=s4.at[0],
+                    send_sem=s4,
                     recv_sem=r4.at[seq],
                     device_id={"sp": sp},
                     device_id_type=MESH,
                 ).wait_recv()
 
-    with jax.named_scope("p_finish"):
-        tiles = [fin[seq] for seq in range(2)]
-        query_state = jnp.concatenate([tile[4:5] for tile in tiles], axis=0)
-        key_state = jnp.concatenate([tile[5:6] for tile in tiles], axis=0)
-        rate = -speed * softplus(u_decay)
-        match = jnp.sum(query * new_k, axis=-1, keepdims=True) * (ceiling * sigmoid(u_strength))
-        mixed = jnp.exp(rate) * (query_state - match * key_state) + match * new_v
-        scale = lax.rsqrt(jnp.mean(mixed * mixed, axis=-1, keepdims=True) + EPS)
-        read = mixed * scale * gains[...]
-        row = iota((8, HD), 0)
-        for seq in range(2):
-            out_ref[seq] = jnp.where(row == 4, read[seq : seq + 1], tiles[seq])
+    aux_copy.wait()
 
 
 def near(a):
     return pltpu.with_memory_space_constraint(a, pltpu.VMEM)
 
 
-def place_outputs(tiles_ref, cache_ref, read_ref):
+def place_outputs(fin_ref, aux_ref, cache_ref, read_ref):
+    tiles = [fin_ref[seq] for seq in range(2)]
     for seq in range(2):
-        cache_ref[seq, 0] = tiles_ref[seq, 0:4].astype(BF16)
-    rows = [tiles_ref[seq, 4:5] for seq in range(2)]
-    read_ref[...] = jnp.concatenate(rows, axis=0).astype(BF16)
+        cache_ref[seq, 0] = tiles[seq][0:4].astype(BF16)
+    query_state = jnp.concatenate([tile[4:5] for tile in tiles], axis=0)
+    key_state = jnp.concatenate([tile[5:6] for tile in tiles], axis=0)
+    mixed = aux_ref[0] * query_state - aux_ref[1] * key_state + aux_ref[2]
+    scale = lax.rsqrt(jnp.mean(mixed * mixed, axis=-1, keepdims=True) + EPS)
+    read_ref[...] = (mixed * scale * aux_ref[3]).astype(BF16)
 
 
 def on_device(x, wk, wv, wq, wf, wu, speeds, ceilings, mult, spike, up, gain):
@@ -514,9 +529,9 @@
     dma = pltpu.SemaphoreType.DMA
     out = pl.pallas_call(
         kernel,
-        out_shape=OUT((seqs, 8, HD), F32),
+        out_shape=(OUT((seqs, 8, HD), F32), OUT((4, seqs, HD), F32)),
         in_specs=[any_space] * 6 + [smem] * 2 + [any_space] * 4,
-        out_specs=vmem,
+        out_specs=(any_space, any_space),
         scratch_shapes=[
             pltpu.VMEM((seqs, span, width), BF16),
             pltpu.VMEM((width, 2 * HD), BF16),
@@ -537,15 +552,15 @@
             pltpu.VMEM((2 * HD, HD), F32),
             pltpu.VMEM((4, 2 * HD, HD), F32),
             pltpu.VMEM((N, 8, HD), F32),
-            pltpu.VMEM((2, 8, HD), F32),
-            dma((3 * NK + 8,)),
+            pltpu.VMEM((4, seqs, HD), F32),
+            dma((NK + 4,)),
+            dma,
             dma((2,)),
-            dma((2,)),
-            dma((2,)),
+            dma,
             dma((4, 2)),
-            dma((2,)),
+            dma,
             dma((4, 2)),
-            dma((N,)),
+            dma,
             dma((2,)),
             pltpu.SemaphoreType.REGULAR,
             pltpu.SemaphoreType.REGULAR,
@@ -571,9 +586,9 @@
             jax.ShapeDtypeStruct((seqs, 1, HD // N, HD), BF16),
             jax.ShapeDtypeStruct((seqs, HD), BF16),
         ),
-        in_specs=[vmem],
+        in_specs=[vmem, vmem],
         out_specs=(vmem, vmem),
-    )(near(out))
+    )(near(out[0]), near(out[1]))
 
 
 def solution(mesh):

time: 33.3 us -> 32.7 us (0.982)
  Pallas kernels: 31.1 us -> 30.6 us
    pallas_call x1, Pallas kernels: 30.5 us -> 30 us  [on_device(): pl.pallas_call(kernel, out_shape=(OUT((seqs, 8, HD), F32), OUT((4, seqs,...]
where the time goes in v5:
time: 32.7 us; the launch traced here: 32.6 us
  Pallas kernels  30.6 us (94%)
  between operations  1.93 us (6%)
    pallas_call x1, Pallas kernels, on_device(): pl.pallas_call(kernel, out_shape=(OUT((seqs, 8, HD), F32), OUT((4, seqs,...  30 us

profile of v5, /device:TPU:6, one launch (start us, length us, event | category | flops | bytes accessed | tf_op | source)
XLA Modules:
  0.0 32.6 jit_solution(12249939395319384787)
XLA Ops:
  1.9 30.0 %shard_map.131 = (f32[2,8,128]{2,1,0:T(8,128)S(1)}, f32[4,2,128]{2,1,0:T(2,128)S(1)}) custom-call(bf16[2,256,2048]{2,1,0:T(8,128)(2,1)} %x_hbm.1, bf16[2048,128]{1,0:T(8,128)(2,1)} %wk_hbm.1, bf16[2048,128]{1,0:T(8,128)(2,1)} %wv_hbm.1, bf16[2048,128]{1,0:T(8,128)(2,1)} %wq_hbm.1, bf16[8,2048]{1,0:T(8,128)(2,1)} %bitcast.5, bf16[8,2048]{1,0:T(8,128)(2,1)} %bitcast.6, ...), custom_call_target="tpu_custom_call" | custom-call | tf_op jit(solution)/shard_map/pallas_call | solution.py:530
  32.0 0.6 %shard_map.132 = (bf16[2,1,4,128]{3,2,1,0:T(4,128)(2,1)}, bf16[2,128]{1,0:T(2,128)(2,1)}) custom-call(f32[2,8,128]{2,1,0:T(8,128)S(1)} %get-tuple-element.4.fin_ref, f32[4,2,128]{2,1,0:T(2,128)S(1)} %get-tuple-element.5.aux_ref), custom_call_target="tpu_custom_call" | custom-call | tf_op jit(solution)/shard_map/pallas_call | solution.py:583

commit v6 on v5

--- a/solution.py
+++ b/solution.py
@@ -67,7 +67,7 @@
     rows, cols = iota((CH, CH), 0), iota((CH, CH), 1)
     c_rows = [jnp.transpose(jnp.broadcast_to(c, (CH, CH))) for c in sums]
     ends = [c[:, CH - 1 :] for c in sums]
-    match = [dot1(k, k, NT) for k in keys]
+    match = [dot3(k, k, NT) for k in keys]
     k_t = [jnp.transpose(k) for k in keys]
     v_t = [jnp.transpose(v) for v in values]
     power = [
@@ -79,11 +79,11 @@
         for i in some
     ]
     for level in range(6):
-        both = [dot1(jnp.concatenate([power[i], rhs[i]], axis=0), power[i]) for i in some]
+        both = [dot3(jnp.concatenate([power[i], rhs[i]], axis=0), power[i]) for i in some]
         power = [both[i][:CH] for i in some]
         applied = [both[i][CH:] for i in some]
         rhs = [rhs[i] - applied[i] if level == 0 else rhs[i] + applied[i] for i in some]
-    rhs = [rhs[i] + dot1(rhs[i], power[i]) for i in some]
+    rhs = [rhs[i] + dot3(rhs[i], power[i]) for i in some]
     faded = [keys[i] * jnp.exp(ends[i] - c_rows[i]) for i in some]
     decayed = [jnp.where(rows == cols, jnp.exp(ends[i]), 0.0) for i in some]
     turned = [dot3(rhs[i][:HD], faded[i]) + decayed[i] for i in some]

time: 32.7 us -> 32.8 us (level)
  no operation moved by 1% of the time
where the time goes in v6:
time: 32.8 us; the launch traced here: 32.5 us
  Pallas kernels  30.6 us (93%)
  between operations  1.93 us (6%)
    pallas_call x1, Pallas kernels, on_device(): pl.pallas_call(kernel, out_shape=(OUT((seqs, 8, HD), F32), OUT((4, seqs,...  30 us

profile of v6, /device:TPU:6, one launch (start us, length us, event | category | flops | bytes accessed | tf_op | source)
XLA Modules:
  0.0 32.5 jit_solution(16590578539589217303)
XLA Ops:
  1.9 30.0 %shard_map.131 = (f32[2,8,128]{2,1,0:T(8,128)S(1)}, f32[4,2,128]{2,1,0:T(2,128)S(1)}) custom-call(bf16[2,256,2048]{2,1,0:T(8,128)(2,1)} %x_hbm.1, bf16[2048,128]{1,0:T(8,128)(2,1)} %wk_hbm.1, bf16[2048,128]{1,0:T(8,128)(2,1)} %wv_hbm.1, bf16[2048,128]{1,0:T(8,128)(2,1)} %wq_hbm.1, bf16[8,2048]{1,0:T(8,128)(2,1)} %bitcast.5, bf16[8,2048]{1,0:T(8,128)(2,1)} %bitcast.6, ...), custom_call_target="tpu_custom_call" | custom-call | tf_op jit(solution)/shard_map/pallas_call | solution.py:530
  31.9 0.6 %shard_map.132 = (bf16[2,1,4,128]{3,2,1,0:T(4,128)(2,1)}, bf16[2,128]{1,0:T(2,128)(2,1)}) custom-call(f32[2,8,128]{2,1,0:T(8,128)S(1)} %get-tuple-element.4.fin_ref, f32[4,2,128]{2,1,0:T(2,128)S(1)} %get-tuple-element.5.aux_ref), custom_call_target="tpu_custom_call" | custom-call | tf_op jit(solution)/shard_map/pallas_call | solution.py:583
